TPU v7x, 32 devices: a whole 2x2x4 slice. The times are simulated.
32 devices in a mesh: sp: 8 (over z, y), tp: 4 (over x, core).
Axes of the slice: x: 2, y: 2, z: 4, core: 2. Of those that a mesh axis runs over, the one named last changes fastest.
Arguments:
- expert_input: bfloat16 [3072, 2048], P('sp'), may hold values from -6 to 6
- cotangent: bfloat16 [3072, 2048], P('sp'), may hold values from -6 to 6
- routes: int32 [3072, 2], P('sp'), may hold values from 0 to 7, all different within a row; in each aligned block of 384 rows (0 to 383, 384 to 767, ...) at most 144 rows name the same one
- route_weight: float32 [3072, 2], P('sp'), may hold values from 0.2 to 2.5
- expert_gate: bfloat16 [8, 2048, 1024], P('sp', None, 'tp'), may hold values from -0.125 to 0.125
- expert_up: bfloat16 [8, 2048, 1024], P('sp', None, 'tp'), may hold values from -0.125 to 0.125
- expert_down: bfloat16 [8, 1024, 2048], P('sp', 'tp'), may hold values from -0.1875 to 0.1875
- conv_out: bfloat16 [3072, 1024], P('sp', 'tp'), may hold values from -14 to 14
- conv_value: bfloat16 [3072, 1024], P('sp', 'tp'), may hold values from -6 to 6
- conv_gate: bfloat16 [3072, 1024], P('sp', 'tp'), may hold values from -6 to 6
- conv_taps: float32 [31, 1024], P(None, 'tp'), may hold values from -1 to 1
- norm_gain: float32 [1024], P('tp'), may hold values from 0.1 to 1.9
- norm_bias: float32 [1024], P('tp'), may hold values from -3 to 3
- out_weight: bfloat16 [1024, 2048], P('tp'), may hold values from -0.1875 to 0.1875
Outputs:
- gate_grad: float32 [8, 2048, 1024], P('sp', None, 'tp')
- up_grad: float32 [8, 2048, 1024], P('sp', None, 'tp')
- down_grad: float32 [8, 1024, 2048], P('sp', 'tp')
- resid_grad: bfloat16 [3072, 2048], P('sp')
- out_weight_grad: float32 [1024, 2048], P('tp', 'sp')
- value_grad: bfloat16 [3072, 1024], P('sp', 'tp')
- gate_in_grad: bfloat16 [3072, 1024], P('sp', 'tp')
Inputs may be any that keep to these rules, and one draw needn't show every extreme that they name: `routes`: each token names 2 different experts. In each aligned block of 384 tokens no expert is named by more than 144 tokens, and in every draw some block has an expert named by exactly 144 tokens.
All inputs are finite; a program needn't handle non-finite values.
Results may differ from a plain program's by a relative error of at most 0.018.
Values may be sent and summed in bfloat16 or wider, within the bound.
No kernel may reach another device: no remote copies, remote signals or barrier semaphores. Data moves between devices by JAX's collectives and lax.ppermute only.
A program may use at most 128 MiB of HBM per device.

v0:
```python
import jax
import jax.numpy as jnp
from jax import lax
from jax.sharding import PartitionSpec as P

norm_eps = 1e-06


def passed_along(value, axis, steps):
    count = lax.axis_size(axis)
    leading, last = (max(0, -steps), min(count, count - steps))
    return lax.ppermute(value, axis, [(source, source + steps) for source in range(leading, last)])


def on_device(
    expert_input,
    cotangent,
    routes,
    route_weight,
    expert_gate,
    expert_up,
    expert_down,
    conv_out,
    conv_value,
    conv_gate,
    conv_taps,
    norm_gain,
    norm_bias,
    out_weight,
):
    sp_count = lax.axis_size("sp")
    tp_count = lax.axis_size("tp")
    tok_rows, model_width = expert_input.shape
    share_cols = model_width // tp_count
    top_count = routes.shape[1]
    local_exp = expert_gate.shape[0]
    experts = local_exp * sp_count
    capacity = 3 * top_count * tok_rows // (2 * experts)
    assigns = tok_rows * top_count
    flat_routes = routes.reshape(assigns)
    onehot = (flat_routes[:, None] == jnp.arange(experts, dtype=jnp.int32)[None, :]).astype(
        jnp.int32
    )
    slot_rank = jnp.sum((jnp.cumsum(onehot, axis=0) - onehot) * onehot, axis=1)
    target = flat_routes * capacity + slot_rank
    slot_ids = (
        jnp.full((experts * capacity,), assigns, jnp.int32)
        .at[target]
        .set(jnp.arange(assigns, dtype=jnp.int32))
    )
    token_of = slot_ids // top_count
    padded_in = jnp.concatenate([expert_input, jnp.zeros((1, model_width), jnp.bfloat16)], axis=0)
    padded_cot = jnp.concatenate([cotangent, jnp.zeros((1, model_width), jnp.bfloat16)], axis=0)
    padded_weight = jnp.concatenate(
        [route_weight.reshape(assigns), jnp.zeros((1,), jnp.float32)], axis=0
    )
    send_rows = padded_in[token_of].reshape(experts, capacity, model_width)
    send_cot = (padded_cot[token_of].astype(jnp.float32) * padded_weight[slot_ids][:, None]).astype(
        jnp.bfloat16
    )
    send_cot = send_cot.reshape(experts, capacity, model_width)
    got_rows, got_cot = (
        lax.all_to_all(send_rows, "sp", split_axis=0, concat_axis=0, tiled=True),
        lax.all_to_all(send_cot, "sp", split_axis=0, concat_axis=0, tiled=True),
    )

    def by_expert(arrived):
        return (
            arrived.reshape(sp_count, local_exp, capacity, model_width)
            .transpose(1, 0, 2, 3)
            .reshape(local_exp, sp_count * capacity, model_width)
        )

    slot_rows = by_expert(got_rows)
    slot_cots = by_expert(got_cot)
    pre_gate = jnp.einsum(
        "lrd,ldf->lrf", slot_rows, expert_gate, preferred_element_type=jnp.float32
    )
    pre_up = jnp.einsum("lrd,ldf->lrf", slot_rows, expert_up, preferred_element_type=jnp.float32)
    gate_sig = jax.nn.sigmoid(pre_gate)
    gate_act = pre_gate * gate_sig
    hidden = (gate_act * pre_up).astype(jnp.bfloat16)
    hidden_grad = jnp.einsum(
        "lrd,lfd->lrf", slot_cots, expert_down, preferred_element_type=jnp.float32
    )
    down_grad = jnp.einsum("lrf,lrd->lfd", hidden, slot_cots, preferred_element_type=jnp.float32)
    gate_pre = (hidden_grad * pre_up * gate_sig * (1.0 + pre_gate * (1.0 - gate_sig))).astype(
        jnp.bfloat16
    )
    up_pre = (hidden_grad * gate_act).astype(jnp.bfloat16)
    gate_grad = jnp.einsum("lrd,lrf->ldf", slot_rows, gate_pre, preferred_element_type=jnp.float32)
    up_grad = jnp.einsum("lrd,lrf->ldf", slot_rows, up_pre, preferred_element_type=jnp.float32)
    partial_rows = jnp.einsum(
        "lrf,ldf->lrd", gate_pre, expert_gate, preferred_element_type=jnp.float32
    )
    partial_rows = partial_rows + jnp.einsum(
        "lrf,ldf->lrd", up_pre, expert_up, preferred_element_type=jnp.float32
    )
    partial_src = (
        partial_rows.reshape(local_exp, sp_count, capacity, model_width)
        .transpose(1, 0, 2, 3)
        .reshape(experts, capacity, model_width)
    )
    partial_low = partial_src.astype(jnp.bfloat16)
    row_share = lax.psum_scatter(partial_low, "tp", scatter_dimension=2, tiled=True).astype(
        jnp.float32
    )
    slot_back = lax.all_to_all(
        row_share.astype(jnp.bfloat16), "sp", split_axis=0, concat_axis=0, tiled=True
    )
    picked = slot_back.reshape(experts * capacity, share_cols)[target].astype(jnp.float32)
    combined = jnp.sum(picked.reshape(tok_rows, top_count, share_cols), axis=1)
    own_cot = lax.dynamic_slice_in_dim(cotangent, lax.axis_index("tp") * share_cols, share_cols, 1)
    resid_part = (own_cot.astype(jnp.float32) + combined).astype(jnp.bfloat16)
    resid_grad = lax.all_gather(resid_part, "tp", axis=1, tiled=True)
    mix_grad = lax.dot_general(
        resid_grad, out_weight, (((1,), (1,)), ((), ())), preferred_element_type=jnp.float32
    )
    channels = conv_out.shape[1] * tp_count
    conv_vals = conv_out.astype(jnp.float32)
    row_sum, row_square = lax.psum(
        (jnp.sum(conv_vals, axis=1), jnp.sum(conv_vals * conv_vals, axis=1)), "tp"
    )
    row_mean = (row_sum / channels)[:, None]
    row_var = (row_square / channels)[:, None] - row_mean * row_mean
    row_rstd = lax.rsqrt(row_var + norm_eps)
    normed = (conv_vals - row_mean) * row_rstd
    norm_pre = normed * norm_gain[None, :] + norm_bias[None, :]
    norm_sig = jax.nn.sigmoid(norm_pre)
    conv_act = (norm_pre * norm_sig).astype(jnp.bfloat16)
    norm_grad = mix_grad * norm_sig * (1.0 + norm_pre * (1.0 - norm_sig)) * norm_gain[None, :]
    grad_sum, grad_dot = lax.psum(
        (jnp.sum(norm_grad, axis=1), jnp.sum(norm_grad * normed, axis=1)), "tp"
    )
    conv_grad = row_rstd * (
        norm_grad - (grad_sum / channels)[:, None] - normed * (grad_dot / channels)[:, None]
    )
    taps_count = conv_taps.shape[0]
    next_rows = passed_along(conv_grad[: taps_count - 1], "sp", -1)
    extended = jnp.concatenate([conv_grad, next_rows], axis=0)
    glu_grad = jnp.zeros_like(conv_grad)
    for lag_index in range(taps_count):
        begin = taps_count - 1 - lag_index
        glu_grad = glu_grad + conv_taps[lag_index][None, :] * extended[begin : begin + tok_rows]
    gate_sig_in = jax.nn.sigmoid(conv_gate.astype(jnp.float32))
    value_grad = (glu_grad * gate_sig_in).astype(jnp.bfloat16)
    gate_in_grad = (
        glu_grad * conv_value.astype(jnp.float32) * gate_sig_in * (1.0 - gate_sig_in)
    ).astype(jnp.bfloat16)
    projected = lax.psum_scatter(
        lax.dot_general(
            resid_grad, conv_act, (((0,), (0,)), ((), ())), preferred_element_type=jnp.float32
        ).astype(jnp.bfloat16),
        "sp",
        scatter_dimension=0,
        tiled=True,
    ).astype(jnp.float32)
    out_weight_grad = projected.T
    return (gate_grad, up_grad, down_grad, resid_grad, out_weight_grad, value_grad, gate_in_grad)


def solution(mesh):
    return jax.shard_map(
        on_device,
        mesh=mesh,
        in_specs=(
            P("sp", None),
            P("sp", None),
            P("sp", None),
            P("sp", None),
            P("sp", None, "tp"),
            P("sp", None, "tp"),
            P("sp", "tp", None),
            P("sp", "tp"),
            P("sp", "tp"),
            P("sp", "tp"),
            P(None, "tp"),
            P("tp"),
            P("tp"),
            P("tp", None),
        ),
        out_specs=(
            P("sp", None, "tp"),
            P("sp", None, "tp"),
            P("sp", "tp", None),
            P("sp", None),
            P("tp", "sp"),
            P("sp", "tp"),
            P("sp", "tp"),
        ),
        check_vma=False,
    )
```

profile of v0, /device:TPU:0, one launch (start us, length us, event | category | flops | bytes accessed | tf_op | source)
XLA Modules:
  0.0 437.1 jit_solution(16315838665781206947)
XLA Ops:
  7.2 0.8 broadcast_multiply_fusion
  8.0 0.8 copy.25
  9.2 0.2 mul.443
  9.4 1.7 reduce-window.6
  11.3 0.2 reduce-window.9
  11.7 3.4 scatter_custom_fusion
  15.1 1.5 concatenate.12
  16.6 6.0 %gather_fusion = bf16[1152,2048]{1,0:T(8,128)(2,1)} fusion(bf16[385,2048]{1,0:T(8,128)(2,1)S(1)} %concatenate.12, s32[2048]{0:T(1024)S(1)} %get-tuple-element.70), kind=kCustom, calls=%fused_computation | custom fusion | bytes 9441792 | tf_op jit(solution)/shard_map/gather | solution.py:57
  22.7 7.3 %all-to-all-start = ((bf16[8,144,2048]{2,1,0:T(8,128)(2,1)}), bf16[8,144,2048]{2,1,0:T(8,128)(2,1)}, u32[]{:S(2)}, u32[]{:S(2)}) async-start(bf16[8,144,2048]{2,1,0:T(8,128)(2,1)} %bitcast.85), calls=%async_computation | async-start | bytes 9437184 | tf_op jit(solution)/shard_map/all_to_all | solution.py:63
  30.0 1.5 concatenate.13
  31.5 5.9 %gather_fusion.1 = bf16[1152,2048]{1,0:T(8,128)(2,1)} fusion(bf16[385,2048]{1,0:T(8,128)(2,1)S(1)} %concatenate.13, s32[2048]{0:T(1024)S(1)} %get-tuple-element.70), kind=kCustom, calls=%fused_computation.1 | custom fusion | bytes 9441792 | tf_op jit(solution)/shard_map/gather | solution.py:58
  37.6 0.1 reshape.160
  37.7 4.6 %gather_fusion.2 = f32[1152]{0:T(1024)S(1)} fusion(f32[769]{0:T(1024)S(1)} %pad_maximum_fusion.1, s32[2048]{0:T(1024)S(1)} %get-tuple-element.69), kind=kCustom, calls=%fused_computation.2 | custom fusion | bytes 13824 | tf_op jit(solution)/shard_map/gather | solution.py:58
  42.4 5.4 %fusion = bf16[8,144,2048]{2,1,0:T(8,128)(2,1)} fusion(bf16[8,144,2048]{2,1,0:T(8,128)(2,1)} %bitcast.87, f32[8,144]{1,0:T(8,128)S(1)} %mul.445), kind=kLoop, calls=%fused_computation.7 | loop fusion | flops 7077888 | bytes 9441792 | tf_op jit(solution)/shard_map/convert_element_type | solution.py:58
  47.8 86.7 %all-to-all-done = bf16[8,144,2048]{2,1,0:T(8,128)(2,1)} async-done(((bf16[8,144,2048]{2,1,0:T(8,128)(2,1)}), bf16[8,144,2048]{2,1,0:T(8,128)(2,1)}, u32[]{:S(2)}, u32[]{:S(2)}) %all-to-all-start) | async-done | bytes 4718624 | tf_op jit(solution)/shard_map/all_to_all | solution.py:63
  134.5 4.6 %all-to-all-start.1 = ((bf16[8,144,2048]{2,1,0:T(8,128)(2,1)}), bf16[8,144,2048]{2,1,0:T(8,128)(2,1)}, u32[]{:S(2)}, u32[]{:S(2)}) async-start(bf16[8,144,2048]{2,1,0:T(8,128)(2,1)} %fusion), calls=%async_computation.1 | async-start | bytes 9437184 | tf_op jit(solution)/shard_map/all_to_all | solution.py:64
  139.1 0.2 reduce-scatter.3.cloned.1.call-start
  139.3 4.8 %fusion.7 = f32[1152,256]{1,0:T(8,128)} fusion(bf16[1152,2048]{1,0:T(8,128)(2,1)} %bitcast.4, bf16[1,2048,256]{2,1,0:T(8,128)(2,1)S(1)} %copy-done), kind=kOutput, calls=%fused_computation.52 | convolution fusion | flops 1207959552 | bytes 6946816 | tf_op jit(solution)/shard_map/lrd,ldf->lrf/dot_general | solution.py:76
  144.2 4.7 %fusion.10 = f32[1152,256]{1,0:T(8,128)} fusion(bf16[1152,2048]{1,0:T(8,128)(2,1)} %bitcast.4, bf16[1,2048,256]{2,1,0:T(8,128)(2,1)S(1)} %copy-done.4), kind=kOutput, calls=%fused_computation.55 | convolution fusion | flops 1207959552 | bytes 6946816 | tf_op jit(solution)/shard_map/lrd,ldf->lrf/dot_general | solution.py:79
  148.9 93.9 %all-to-all-done.1 = bf16[8,144,2048]{2,1,0:T(8,128)(2,1)} async-done(((bf16[8,144,2048]{2,1,0:T(8,128)(2,1)}), bf16[8,144,2048]{2,1,0:T(8,128)(2,1)}, u32[]{:S(2)}, u32[]{:S(2)}) %all-to-all-start.1) | async-done | bytes 4718624 | tf_op jit(solution)/shard_map/all_to_all | solution.py:64
  242.8 5.0 %multiply_convert_fusion.1 = (bf16[1152,256]{1,0:T(8,128)(2,1)S(1)}, bf16[1152,256]{1,0:T(8,128)(2,1)S(1)}) fusion(f32[1152,256]{1,0:T(8,128)} %fusion.7, f32[1152,256]{1,0:T(8,128)} %fusion.10, bf16[1152,2048]{1,0:T(8,128)(2,1)} %bitcast.6, bf16[1,256,2048]{2,1,0:T(8,128)(2,1)} %param.20), kind=kOutput, calls=%fused_computation.46 | convolution fusion | flops 1211793408 | bytes 9306112 | tf_op jit(solution)/shard_map/lrd,lfd->lrf/dot_general | solution.py:83
  247.9 1.4 fusion.5
  249.3 3.7 fusion.1
  253.0 47.0 %reduce-scatter.3.cloned.1.call-done = bf16[8,144,512]{2,1,0:T(8,128)(2,1)} async-done(((bf16[8,144,2048]{2,1,0:T(8,128)(2,1)}), bf16[8,144,512]{2,1,0:T(8,128)(2,1)}) %reduce-scatter.3.cloned.1.call-update) | async-done | bytes 1179664 | tf_op jit(solution)/shard_map/reduce_scatter | solution.py:105
  300.1 5.5 %all-to-all-start.2 = ((bf16[8,144,512]{2,1,0:T(8,128)(2,1)}), bf16[8,144,512]{2,1,0:T(8,128)(2,1)S(1)}, u32[]{:S(2)}, u32[]{:S(2)}) async-start(bf16[8,144,512]{2,1,0:T(8,128)(2,1)} %reduce-scatter.3.cloned.1.call-done), calls=%async_computation.3 | async-start | bytes 2359296 | tf_op jit(solution)/shard_map/all_to_all | solution.py:108
  305.7 28.3 %all-to-all-done.2 = bf16[8,144,512]{2,1,0:T(8,128)(2,1)S(1)} async-done(((bf16[8,144,512]{2,1,0:T(8,128)(2,1)}), bf16[8,144,512]{2,1,0:T(8,128)(2,1)S(1)}, u32[]{:S(2)}, u32[]{:S(2)}) %all-to-all-start.2) | async-done | bytes 1179680 | tf_op jit(solution)/shard_map/all_to_all | solution.py:108
  334.0 2.7 gather_fusion.3
  336.7 1.0 reshape.167
  337.6 1.9 reduce_sum.58
  339.6 2.0 add_convert_fusion
  341.6 0.2 convert_reduce_fusion
  341.8 6.2 %all-reduce.3 = (f32[384]{0:T(512)S(1)}, f32[384]{0:T(512)S(1)}) all-reduce(f32[384]{0:T(512)S(1)} %get-tuple-element.24, f32[384]{0:T(512)S(1)} %get-tuple-element.23), channel_id=1, replica_groups=mesh['sp'=8,'tp'=4] {'tp'}, use_global_device_ids=true, to_apply=%region_9.10 | all-reduce | flops 768 | bytes 6144 | tf_op jit(solution)/shard_map/psum | solution.py:121
  348.1 5.4 %convolution_bitcast_fusion.2 = f32[1,2048,256]{2,1,0:T(8,128)} fusion(bf16[1152,2048]{1,0:T(8,128)(2,1)} %bitcast.4, bf16[1152,256]{1,0:T(8,128)(2,1)S(1)} %copy-done.3), kind=kOutput, calls=%fused_computation.40 | convolution fusion | flops 1207959552 | bytes 7405568 | tf_op jit(solution)/shard_map/lrd,lrf->ldf/dot_general | solution.py:91
  353.5 5.4 %convolution_bitcast_fusion = f32[1,256,2048]{2,1,0:T(8,128)} fusion(bf16[1152,2048]{1,0:T(8,128)(2,1)} %bitcast.6, f32[1152,256]{1,0:T(8,128)S(1)} %copy-done.16, f32[1152,256]{1,0:T(8,128)S(1)} %copy-done.15), kind=kOutput, calls=%fused_computation.38 | convolution fusion | flops 1209729024 | bytes 9175040 | tf_op jit(solution)/shard_map/lrf,lrd->lfd/dot_general | solution.py:86
  358.8 0.6 all-gather.2.cloned.1.call-done
  359.5 3.4 convolution_convert_fusion
  362.9 2.7 fusion.137
  365.6 6.4 %all-reduce.2 = (f32[384]{0:T(512)}, f32[384]{0:T(512)S(1)}) all-reduce(f32[384]{0:T(512)S(1)} %get-tuple-element.22, f32[384]{0:T(512)S(1)} %get-tuple-element.21), channel_id=1, replica_groups=mesh['sp'=8,'tp'=4] {'tp'}, use_global_device_ids=true, to_apply=%region_14.15 | all-reduce | flops 768 | bytes 6144 | tf_op jit(solution)/shard_map/psum | solution.py:132
  372.0 0.7 broadcast_multiply_fusion.1
  372.7 1.3 fusion.29
  374.0 1.4 collective-permute-start
  375.5 5.2 %convolution_bitcast_fusion.1 = f32[1,2048,256]{2,1,0:T(8,128)} fusion(bf16[1152,2048]{1,0:T(8,128)(2,1)} %bitcast.4, bf16[1152,256]{1,0:T(8,128)(2,1)S(1)} %copy-done.9), kind=kOutput, calls=%fused_computation.39 | convolution fusion | flops 1207959552 | bytes 7405568 | tf_op jit(solution)/shard_map/lrd,lrf->ldf/dot_general | solution.py:92
  380.7 2.7 multiply_convert_fusion.4
  383.5 0.8 multiply_convert_fusion.5
  384.2 43.5 %reduce-scatter.5.cloned.1.call-done = bf16[256,256]{1,0:T(8,128)(2,1)} async-done(((bf16[2048,256]{1,0:T(8,128)(2,1)}), bf16[256,256]{1,0:T(8,128)(2,1)}) %reduce-scatter.5.cloned.1.call-update) | async-done | bytes 131088 | tf_op jit(solution)/shard_map/reduce_scatter | solution.py:150
  427.7 0.9 convert_bitcast_fusion
  428.6 0.8 copy.30
  429.5 1.1 copy.32
  (61 shorter events, 1.4 us)
Async XLA Ops:
  7.2 132.2 %copy-start = (bf16[1,2048,256]{2,1,0:T(8,128)(2,1)S(1)}, bf16[1,2048,256]{2,1,0:T(8,128)(2,1)}, u32[]{:S(2)}) copy-start(bf16[1,2048,256]{2,1,0:T(8,128)(2,1)} %param.18) | copy-start | bytes 3145732
  22.7 111.8 %all-to-all-start = ((bf16[8,144,2048]{2,1,0:T(8,128)(2,1)}), bf16[8,144,2048]{2,1,0:T(8,128)(2,1)}, u32[]{:S(2)}, u32[]{:S(2)}) async-start(bf16[8,144,2048]{2,1,0:T(8,128)(2,1)} %bitcast.85), calls=%async_computation | async-start | bytes 9437184 | tf_op jit(solution)/shard_map/all_to_all | solution.py:63
  31.5 5.9 %copy-start.12 = (f32[384,2]{0,1:T(2,128)S(1)}, f32[384,2]{0,1:T(2,128)}, u32[]{:S(2)}) copy-start(f32[384,2]{0,1:T(2,128)} %param.17) | copy-start | bytes 9220
  134.5 108.3 %all-to-all-start.1 = ((bf16[8,144,2048]{2,1,0:T(8,128)(2,1)}), bf16[8,144,2048]{2,1,0:T(8,128)(2,1)}, u32[]{:S(2)}, u32[]{:S(2)}) async-start(bf16[8,144,2048]{2,1,0:T(8,128)(2,1)} %fusion), calls=%async_computation.1 | async-start | bytes 9437184 | tf_op jit(solution)/shard_map/all_to_all | solution.py:64
  139.1 161.0 %reduce-scatter.3.cloned.1.call-start = ((), (), s32[]{:S(2)}) async-start(), calls=%async_computation.5 | async-start | bytes 5898240 | tf_op jit(solution)/shard_map/reduce_scatter | solution.py:105
  139.3 4.8 %copy-start.4 = (bf16[1,2048,256]{2,1,0:T(8,128)(2,1)S(1)}, bf16[1,2048,256]{2,1,0:T(8,128)(2,1)}, u32[]{:S(2)}) copy-start(bf16[1,2048,256]{2,1,0:T(8,128)(2,1)} %param.19) | copy-start | bytes 3145732
  247.9 1.5 copy-start.2
  247.9 1.5 copy-start.8
  300.1 33.9 %all-to-all-start.2 = ((bf16[8,144,512]{2,1,0:T(8,128)(2,1)}), bf16[8,144,512]{2,1,0:T(8,128)(2,1)S(1)}, u32[]{:S(2)}, u32[]{:S(2)}) async-start(bf16[8,144,512]{2,1,0:T(8,128)(2,1)} %reduce-scatter.3.cloned.1.call-done), calls=%async_computation.3 | async-start | bytes 2359296 | tf_op jit(solution)/shard_map/all_to_all | solution.py:108
  305.6 53.9 %all-gather.2.cloned.1.call-start = ((), (), s32[]{:S(2)}) async-start(), calls=%async_computation.6 | async-start | bytes 1966080 | tf_op jit(solution)/shard_map/all_gather | solution.py:115
  339.5 2.1 copy-start.6
  339.5 8.5 %copy-start.11 = (f32[31,256]{1,0:T(8,128)S(1)}, f32[31,256]{1,0:T(8,128)}, u32[]{:S(2)}) copy-start(f32[31,256]{1,0:T(8,128)} %param.24) | copy-start | bytes 95236
  339.5 8.5 %copy-start.3 = (bf16[1152,256]{1,0:T(8,128)(2,1)S(1)}, bf16[1152,256]{1,0:T(8,128)(2,1)}, u32[]{:S(2)}) copy-start(bf16[1152,256]{1,0:T(8,128)(2,1)} %copy-done.2) | copy-start | bytes 1769476
  341.5 86.2 %reduce-scatter.5.cloned.1.call-start = ((), (), s32[]{:S(2)}) async-start(), calls=%async_computation.7 | async-start | bytes 1179648 | tf_op jit(solution)/shard_map/reduce_scatter | solution.py:150
  348.0 5.4 %copy-start.15 = (f32[1152,256]{1,0:T(8,128)S(1)}, f32[1152,256]{1,0:T(8,128)}, u32[]{:S(2)}) copy-start(f32[1152,256]{1,0:T(8,128)} %fusion.7) | copy-start | bytes 3538948
  348.1 5.4 %copy-start.16 = (f32[1152,256]{1,0:T(8,128)S(1)}, f32[1152,256]{1,0:T(8,128)}, u32[]{:S(2)}) copy-start(f32[1152,256]{1,0:T(8,128)} %fusion.10) | copy-start | bytes 3538948
  353.4 6.0 %copy-start.7 = (bf16[384,256]{1,0:T(8,128)(2,1)S(1)}, bf16[384,256]{1,0:T(8,128)(2,1)}, u32[]{:S(2)}) copy-start(bf16[384,256]{1,0:T(8,128)(2,1)} %param.21) | copy-start | bytes 589828
  353.4 6.0 %copy-start.13 = (f32[256]{0:T(256)S(1)}, f32[256]{0:T(256)}, u32[]{:S(2)}) copy-start(f32[256]{0:T(256)} %param.26) | copy-start | bytes 3076
  353.5 6.0 %copy-start.14 = (f32[256]{0:T(256)S(1)}, f32[256]{0:T(256)}, u32[]{:S(2)}) copy-start(f32[256]{0:T(256)} %param.25) | copy-start | bytes 3076
  359.5 3.4 copy-start.1
  362.9 12.5 %copy-start.9 = (bf16[1152,256]{1,0:T(8,128)(2,1)S(1)}, bf16[1152,256]{1,0:T(8,128)(2,1)}, u32[]{:S(2)}) copy-start(bf16[1152,256]{1,0:T(8,128)(2,1)} %copy-done.8) | copy-start | bytes 1769476
  374.0 6.7 %copy-start.5 = (bf16[384,256]{1,0:T(8,128)(2,1)S(1)}, bf16[384,256]{1,0:T(8,128)(2,1)}, u32[]{:S(2)}) copy-start(bf16[384,256]{1,0:T(8,128)(2,1)} %param.23) | copy-start | bytes 589828
  374.0 6.7 %copy-start.10 = (bf16[384,256]{1,0:T(8,128)(2,1)S(1)}, bf16[384,256]{1,0:T(8,128)(2,1)}, u32[]{:S(2)}) copy-start(bf16[384,256]{1,0:T(8,128)(2,1)} %param.22) | copy-start | bytes 589828
  374.0 6.7 %collective-permute-start = (f32[30,256]{1,0:T(8,128)S(1)}, f32[30,256]{1,0:T(8,128)S(1)}, u32[]{:S(2)}, u32[]{:S(2)}) collective-permute-start(f32[30,256]{1,0:T(8,128)S(1)} %slice.265), channel_id=1, source_target_pairs={{4,0},{8,4},{12,8},{16,12},{20,16},{24,20},{28,24},{5,1},{9,5},{13... | collective-permute-start | bytes 92168 | tf_op jit(solution)/shard_map/ppermute | solution.py:12
Sparse Core Ops, SparseCore 0:
  253.2 46.8 reduce-scatter.2
  341.7 17.7 all-gather.1
  363.4 64.2 reduce-scatter.4
where the time goes:
time: 438 us; the launch traced here: 437 us
  waiting for transfers between devices  300 us (68%)
  matrix products  41.8 us (10%)
  local copies, waits for them, and re-layouts  30.7 us (7%)
  starting transfers between devices  19.1 us (4%)
  other arithmetic  18.6 us (4%)
  between operations  14.2 us (3%)
  blocking collectives  12.6 us (3%)
    all_to_all x1, waiting for transfers between devices, on_device(): lax.all_to_all(send_cot, 'sp', split_axis=0, concat_axis=0, tiled=True)  93.9 us
    all_to_all x1, waiting for transfers between devices, on_device(): lax.all_to_all(send_rows, 'sp', split_axis=0, concat_axis=0, tiled=True)  86.7 us
    reduce_scatter x1, waiting for transfers between devices, on_device(): lax.psum_scatter(partial_low, 'tp', scatter_dimension=2, tiled=True)  47 us
    reduce_scatter x1, waiting for transfers between devices, on_device(): lax.psum_scatter(lax.dot_general(resid_grad, conv_act, (((0,), (0,)), (()...  43.5 us
    all_to_all x1, waiting for transfers between devices, on_device(): lax.all_to_all(row_share.astype(jnp.bfloat16), 'sp', split_axis=0, concat...  28.3 us
  transfers between devices with their start and end apart: 7, of which 6 were waited for; matrix products, arithmetic and copies ran while one was open for 12% of the time, Pallas kernels for 0%

commit v1 on v0

v1 whole, which is shorter than its diff:
```python
import functools
import math

import jax
import jax.numpy as jnp
from jax import lax
from jax.experimental import pallas as pl
from jax.experimental.pallas import tpu as pltpu
from jax.sharding import PartitionSpec as P


norm_eps = 1e-06
f32 = jnp.float32
bf16 = jnp.bfloat16


def mm(a, b, ca, cb):
    return lax.dot_general(a, b, (((ca,), (cb,)), ((), ())), preferred_element_type=f32)


def exact_mm(a, b, ca, cb):
    return lax.dot_general(
        a, b, (((ca,), (cb,)), ((), ())), preferred_element_type=f32, precision=lax.Precision.HIGHEST
    )


def params(blocks, copies):
    if copies == 0:
        return pltpu.CompilerParams(vmem_limit_bytes=56 * 1024 * 1024)
    need = sum(math.prod(shape) * jnp.dtype(kind).itemsize for shape, kind in blocks)
    return pltpu.CompilerParams(vmem_limit_bytes=copies * need + 8 * 1024 * 1024)


def tp_swap(value, dist):
    count = lax.axis_size("tp")
    return lax.ppermute(value, "tp", [(i, i ^ dist) for i in range(count)])


def tp_pieces(own):
    far = tp_swap(own, 2)
    return (own, tp_swap(own, 1), far, tp_swap(far, 1))


def passed_along(value, axis, steps):
    count = lax.axis_size(axis)
    leading, last = (max(0, -steps), min(count, count - steps))
    return lax.ppermute(value, axis, [(source, source + steps) for source in range(leading, last)])


def dispatch_body(at_ref, routes_ref, weight_ref, source_ref, *outs, cots):
    experts, capacity = len(outs), outs[0].shape[0]
    top, tokens = routes_ref.shape
    expert_id = lax.broadcasted_iota(jnp.int32, (experts, tokens), 0)
    named = jnp.zeros((experts, tokens), f32)
    weights = jnp.zeros((experts, tokens), f32)
    for k in range(top):
        hit = (routes_ref[k : k + 1, :] ^ at_ref[1]) == expert_id
        named = jnp.where(hit, 1.0, named)
        weights = jnp.where(hit, weight_ref[k : k + 1, :], weights)
    before = lax.broadcasted_iota(jnp.int32, (tokens, tokens), 0) < lax.broadcasted_iota(
        jnp.int32, (tokens, tokens), 1
    )
    rank = mm(named.astype(bf16), jnp.where(before, 1.0, 0.0).astype(bf16), 1, 0)
    key = jnp.where(named > 0.5, rank, -1.0).astype(jnp.int32)
    slot = lax.broadcasted_iota(jnp.int32, (capacity, tokens), 0)
    for e in range(experts):
        pick = slot == key[e : e + 1, :]
        rows = mm(jnp.where(pick, 1.0, 0.0).astype(bf16), source_ref[...], 1, 0)
        if cots:
            rows = rows * jnp.sum(jnp.where(pick, weights[e : e + 1, :], 0.0), axis=1, keepdims=True)
        outs[e][...] = rows.astype(bf16)


def whole_spec(shape):
    return pl.BlockSpec(shape, lambda i, at: (0,) * len(shape))


def quarter_spec(tokens, share):
    return pl.BlockSpec((tokens, share), lambda i, at: (0, at[0]))


def call(body, at, args, outs, in_specs=None, out_specs=None, steps=1, keep=True):
    in_specs = in_specs or [whole_spec(a.shape) for a in args]
    out_specs = out_specs or [whole_spec(s) for s, _ in outs]
    blocks = [(spec.block_shape, a.dtype) for spec, a in zip(in_specs, args)]
    blocks += [(spec.block_shape, kind) for spec, (_, kind) in zip(out_specs, outs)]
    return pl.pallas_call(
        body,
        grid_spec=pltpu.PrefetchScalarGridSpec(
            num_scalar_prefetch=1, grid=(steps,), in_specs=in_specs, out_specs=out_specs
        ),
        out_shape=[jax.ShapeDtypeStruct(s, d) for s, d in outs],
        compiler_params=params(blocks, keep * min(steps, 2)),
    )(at, *args)


def dispatch(at, routes_t, weight_t, source, experts, capacity, share, cots):
    outs = [((capacity, share), bf16)] * experts
    return call(
        functools.partial(dispatch_body, cots=cots),
        at,
        (routes_t, weight_t, source),
        outs,
        [whole_spec(routes_t.shape), whole_spec(weight_t.shape), quarter_spec(source.shape[0], share)],
        keep=cots,
    )


def sp_swap(value, dist):
    count = lax.axis_size("sp")
    return lax.ppermute(value, "sp", [(i, i ^ dist) for i in range(count)])


def sp_exchange(blocks):
    got = list(blocks)
    for k in range(1, len(blocks)):
        got[k] = sp_swap(blocks[k], k)
    return got


def sp_all(value):
    return lax.all_to_all(value, "sp", split_axis=0, concat_axis=0, tiled=True)


def join(blocks):
    return jnp.concatenate(blocks, axis=0)


def rows_of(ref):
    return join([ref[i] for i in range(ref.shape[0])])


def store_blocks(ref, value, first=0, count=None):
    capacity = ref.shape[1]
    for i in range(ref.shape[0] if count is None else count):
        ref[first + i] = value[i * capacity : (i + 1) * capacity]


def pre_body(at_ref, p0, p1, p2, p3, wg_ref, wu_ref, gate_ref, up_ref):
    share = p0.shape[2]
    gate, up = 0.0, 0.0
    for j, piece in enumerate((p0, p1, p2, p3)):
        at = pl.ds(pl.multiple_of((at_ref[0] ^ j) * share, share), share)
        rows = rows_of(piece)
        gate = gate + mm(rows, wg_ref[at, :], 1, 0)
        up = up + mm(rows, wu_ref[at, :], 1, 0)
    store_blocks(gate_ref, gate)
    store_blocks(up_ref, up)


def blocked(shape):
    return pl.BlockSpec((2, *shape[1:]), lambda i, at: (i, 0, 0))


def pre_acts(at, pieces, w_gate, w_up):
    count, capacity, _ = pieces[0].shape
    mid = (count, capacity, w_gate.shape[1])
    return call(
        pre_body,
        at,
        (*pieces, w_gate, w_up),
        [(mid, f32)] * 2,
        [blocked(pieces[0].shape)] * 4 + [whole_spec(w_gate.shape)] * 2,
        [blocked(mid)] * 2,
        count // 2,
    )


def hidden_body(at_ref, p0, p1, p2, p3, wd_ref, gate_ref, up_ref, hid_ref, gp_ref, up_out_ref):
    share = p0.shape[2]
    grad = 0.0
    for j, piece in enumerate((p0, p1, p2, p3)):
        at = pl.ds(pl.multiple_of((at_ref[0] ^ j) * share, share), share)
        grad = grad + mm(rows_of(piece), wd_ref[:, at], 1, 1)
    gate = rows_of(gate_ref)
    up = rows_of(up_ref)
    sig = jax.nn.sigmoid(gate)
    act = gate * sig
    store_blocks(hid_ref, (act * up).astype(bf16))
    store_blocks(gp_ref, (grad * up * sig * (1.0 + gate * (1.0 - sig))).astype(bf16))
    store_blocks(up_out_ref, (grad * act).astype(bf16))


def hidden_grads(at, pieces, w_down, gate, up):
    count, capacity, _ = pieces[0].shape
    mid = (count, capacity, w_down.shape[0])
    return call(
        hidden_body,
        at,
        (*pieces, w_down, gate, up),
        [(mid, bf16)] * 3,
        [blocked(pieces[0].shape)] * 4 + [whole_spec(w_down.shape)] + [blocked(mid)] * 2,
        [blocked(mid)] * 3,
        count // 2,
    )


def chunk_parts(share, eighth, chunk, chunks):
    sub = eighth // chunks
    return [(b * eighth + chunk * sub, sub) for b in range(share // eighth)]


def slot_body(at_ref, gp_ref, up_ref, wg_ref, wu_ref, *outs, parts):
    share = wg_ref.shape[0] // 4
    count = gp_ref.shape[0]
    gp = rows_of(gp_ref)
    up = rows_of(up_ref)
    for c, spans in enumerate(parts):
        own_ref, near_ref, far_ref = outs[3 * c : 3 * c + 3]
        for j, out, first in ((3, near_ref, 0), (2, far_ref, 0), (1, near_ref, count), (0, own_ref, 0)):
            base = (at_ref[0] ^ j) * share
            rows = [pl.ds(pl.multiple_of(base + lo, size), size) for lo, size in spans]
            part = mm(gp, join([wg_ref[r, :] for r in rows]), 1, 1)
            part = part + mm(up, join([wu_ref[r, :] for r in rows]), 1, 1)
            store_blocks(out, part.astype(bf16), first, count)


def slot_grads(at, gate_pre, up_pre, w_gate, w_up, parts):
    count, capacity, _ = gate_pre.shape
    cols = sum(size for _, size in parts[0])
    one, two = (count, capacity, cols), (2 * count, capacity, cols)
    return call(
        functools.partial(slot_body, parts=parts),
        at,
        (gate_pre, up_pre, w_gate, w_up),
        [(one, bf16), (two, bf16), (one, bf16)] * len(parts),
    )


def add_body(at_ref, *refs, groups):
    ins, outs = refs[: 3 * groups], refs[3 * groups :]
    for g in range(groups):
        own, near, far = ins[3 * g : 3 * g + 3]
        count = own.shape[0]
        for i in range(count):
            total = own[i].astype(f32) + near[count + i].astype(f32) + far[i].astype(f32)
            outs[g * count + i][...] = total.astype(bf16)


def wide_body(at_ref, *refs, groups):
    pieces, sides, out_ref = refs[: 4 * groups], refs[4 * groups : 5 * groups], refs[5 * groups]
    share = pieces[0].shape[2]
    side = join([rows_of(ref) for ref in sides])
    for j in range(4):
        at = pl.ds(pl.multiple_of((at_ref[0] ^ j) * share, share), share)
        rows = join([rows_of(pieces[4 * g + j]) for g in range(groups)])
        out_ref[at, :] = mm(rows, side, 0, 0)


def down_body(at_ref, *refs, groups):
    pieces, hids, dg_ref = refs[: 4 * groups], refs[4 * groups : 5 * groups], refs[5 * groups]
    share = pieces[0].shape[2]
    hid = join([rows_of(ref) for ref in hids])
    for j in range(4):
        at = pl.ds(pl.multiple_of((at_ref[0] ^ j) * share, share), share)
        rows = join([rows_of(pieces[4 * g + j]) for g in range(groups)])
        dg_ref[:, at] = mm(hid, rows, 0, 0)


def picks_body(at_ref, routes_ref, out_ref):
    experts, tokens, capacity = out_ref.shape
    top = routes_ref.shape[1]
    expert_id = lax.broadcasted_iota(jnp.int32, (tokens, experts), 1)
    named = jnp.zeros((tokens, experts), f32)
    for k in range(top):
        named = jnp.where((routes_ref[:, k : k + 1] ^ at_ref[1]) == expert_id, 1.0, named)
    before = lax.broadcasted_iota(jnp.int32, (tokens, tokens), 1) < lax.broadcasted_iota(
        jnp.int32, (tokens, tokens), 0
    )
    rank = mm(jnp.where(before, 1.0, 0.0).astype(bf16), named.astype(bf16), 1, 0)
    key = jnp.where(named > 0.5, rank, -1.0).astype(jnp.int32)
    slot = lax.broadcasted_iota(jnp.int32, (tokens, capacity), 1)
    for e in range(experts):
        out_ref[e] = jnp.where(slot == key[:, e : e + 1], 1.0, 0.0).astype(bf16)


def combine_body(at_ref, picks_ref, cot_ref, *refs, parts):
    backs, out_ref = refs[:-1], refs[-1]
    total = 0.0
    for e in range(picks_ref.shape[0]):
        total = total + mm(picks_ref[e], backs[e][...], 1, 0)
    cot = jnp.concatenate([cot_ref[:, lo : lo + size] for lo, size in parts], axis=1)
    out_ref[...] = (cot.astype(f32) + total).astype(bf16)


def combine(at, picks, cotangent, back, parts, share):
    tokens = cotangent.shape[0]
    (out,) = call(
        functools.partial(combine_body, parts=parts),
        at,
        (picks, cotangent, *back),
        [((tokens, back[0].shape[-1]), bf16)],
        [whole_spec(picks.shape), quarter_spec(tokens, share)] + [whole_spec(b.shape) for b in back],
    )
    return out


def stats_body(at_ref, conv_ref, out_ref):
    vals = conv_ref[...].astype(f32)
    mean = jnp.mean(vals, axis=1, keepdims=True)
    ones = jnp.ones((2, vals.shape[1]), f32)
    means = exact_mm(ones, vals, 1, 1) * (1.0 / vals.shape[1])
    squares = exact_mm(ones, (vals - mean) ** 2, 1, 1)
    row = lax.broadcasted_iota(jnp.int32, means.shape, 0)
    out_ref[...] = jnp.where(row == 0, means, squares)


def moments_body(at_ref, *refs, chan):
    stats, out_ref = [ref[...] for ref in refs[:-1]], refs[-1]
    count = len(stats)
    mean = sum(s[0:1] for s in stats) / count
    m2 = sum(s[1:2] + chan * (s[0:1] - mean) ** 2 for s in stats)
    rstd = lax.rsqrt(m2 / (count * chan) + norm_eps)
    row = lax.broadcasted_iota(jnp.int32, (2, mean.shape[1]), 0)
    both = jnp.where(row == 0, mean, rstd)
    out_ref[...] = exact_mm(both, jnp.eye(2, dtype=f32), 0, 0)


def norm_parts(conv_ref, mean_ref, gain_ref, bias_ref):
    normed = (conv_ref[...].astype(f32) - mean_ref[:, 0:1]) * mean_ref[:, 1:2]
    pre = normed * gain_ref[...] + bias_ref[...]
    sig = jax.nn.sigmoid(pre)
    return normed, pre, sig


def mix_body(at_ref, *refs, parts):
    pieces, refs = refs[: 4 * len(parts)], refs[4 * len(parts) :]
    w_ref, conv_ref, mean_ref, gain_ref, bias_ref, resid_ref, ng_ref, sums_ref = refs
    share = resid_ref.shape[1] // 4
    for c, spans in enumerate(parts):
        for j in range(4):
            base = (at_ref[0] ^ j) * share
            rows = pieces[4 * c + j]
            if len(parts) == 1:
                resid_ref[:, pl.ds(pl.multiple_of(base, share), share)] = rows[...]
                continue
            for b, (lo, size) in enumerate(spans):
                at = pl.ds(pl.multiple_of(base + lo, size), size)
                resid_ref[:, at] = rows[:, b * size : (b + 1) * size]
    mix = mm(resid_ref[...], w_ref[...], 1, 1)
    normed, pre, sig = norm_parts(conv_ref, mean_ref, gain_ref, bias_ref)
    grad = mix * sig * (1.0 + pre * (1.0 - sig)) * gain_ref[...]
    ng_ref[...] = grad
    ones = jnp.ones((2, grad.shape[1]), f32)
    total = exact_mm(ones, grad, 1, 1)
    dot = exact_mm(ones, grad * normed, 1, 1)
    row = lax.broadcasted_iota(jnp.int32, total.shape, 0)
    sums_ref[...] = jnp.where(row == 0, total, dot)


def gates_body(at_ref, value_ref, gate_ref, a_ref, b_ref):
    sig = jax.nn.sigmoid(gate_ref[...].astype(f32))
    a_ref[...] = sig
    b_ref[...] = value_ref[...].astype(f32) * sig * (1.0 - sig)


def owg_body(at_ref, p0, p1, p2, p3, conv_ref, mean_ref, gain_ref, bias_ref, out_ref):
    blocks, _, cols = out_ref.shape
    per = blocks // 4
    _, pre, sig = norm_parts(conv_ref, mean_ref, gain_ref, bias_ref)
    act = (pre * sig).astype(bf16)
    for j, piece in enumerate((p0, p1, p2, p3)):
        part = mm(act, piece[...], 0, 0).astype(bf16)
        for b in range(per):
            out_ref[(at_ref[0] ^ j) * per + b] = part[:, b * cols : (b + 1) * cols]


def on_device(
    expert_input,
    cotangent,
    routes,
    route_weight,
    expert_gate,
    expert_up,
    expert_down,
    conv_out,
    conv_value,
    conv_gate,
    conv_taps,
    norm_gain,
    norm_bias,
    out_weight,
):
    sp_count = lax.axis_size("sp")
    tp_count = lax.axis_size("tp")
    assert tp_count == 4 and expert_gate.shape[0] == 1
    tok_rows, model_width = expert_input.shape
    share = model_width // tp_count
    eighth = model_width // sp_count
    top_count = routes.shape[1]
    experts = sp_count
    capacity = 3 * top_count * tok_rows // (2 * experts)
    w_gate, w_up, w_down = expert_gate[0], expert_up[0], expert_down[0]
    width = w_gate.shape[1]
    chan = conv_out.shape[1]
    channels = chan * tp_count
    at = jnp.stack([lax.axis_index("tp"), lax.axis_index("sp")]).astype(jnp.int32)

    routes_t, weight_t = routes.T, route_weight.T
    sent = (experts, capacity, share)
    got_rows = sp_exchange(dispatch(at, routes_t, weight_t, expert_input, *sent, False))
    send_cots = dispatch(at, routes_t, weight_t, cotangent, *sent, True)
    got_cots = sp_exchange(send_cots)

    (picks,) = call(picks_body, at, (routes,), [((experts, tok_rows, capacity), bf16)])
    (own_stat,) = call(stats_body, at, (conv_out,), [((2, tok_rows), f32)])
    stats = [own_stat] + [tp_swap(own_stat, d) for d in (1, 2, 3)]
    value_scale, gate_scale = call(
        gates_body, at, (conv_value, conv_gate), [((tok_rows, chan), f32)] * 2
    )
    (mean_rstd,) = call(
        functools.partial(moments_body, chan=chan), at, stats, [((tok_rows, 2), f32)]
    )
    row_mean, row_rstd = mean_rstd[:, 0:1], mean_rstd[:, 1:2]
    norm_args = (conv_out, mean_rstd, norm_gain[None, :], norm_bias[None, :])

    half = experts // 2
    row_groups, cot_groups, pre, acts = [], [], [], []
    for g in range(2):
        row_groups.append(tp_pieces(jnp.stack(got_rows[g * half : (g + 1) * half])))
    for g in range(2):
        pre.append(pre_acts(at, row_groups[g], w_gate, w_up))
    for g in range(2):
        cot_groups.append(tp_pieces(jnp.stack(got_cots[g * half : (g + 1) * half])))
    for g in range(2):
        acts.append(hidden_grads(at, cot_groups[g], w_down, *pre[g]))
    hiddens, gate_pres, up_pres = ([a[i] for a in acts] for i in range(3))

    chunks = 2 if eighth % 256 == 0 else 1
    parts = [chunk_parts(share, eighth, c, chunks) for c in range(chunks)]
    cols = share // chunks
    resid_pieces, arrived = [], []
    sums = [[None, None] for _ in range(chunks)]
    for g in range(2):
        slots = slot_grads(at, gate_pres[g], up_pres[g], w_gate, w_up, parts)
        for c in range(chunks):
            own, near, far = slots[3 * c : 3 * c + 3]
            near = tp_swap(near, 1)
            far = (far.astype(f32) + near[:half].astype(f32)).astype(bf16)
            sums[c][g] = (own, near, tp_swap(far, 2))
    backs = []
    add = functools.partial(add_body, groups=2)
    for c in range(chunks):
        args = (*sums[c][0], *sums[c][1])
        totals = call(add, at, args, [((capacity, cols), bf16)] * experts)
        backs.append(sp_exchange(totals))
    wide = []
    for sides in (gate_pres, up_pres):
        wide += call(
            functools.partial(wide_body, groups=2),
            at,
            (*row_groups[0], *row_groups[1], *sides),
            [((model_width, width), f32)],
        )
    gate_grad, up_grad = wide
    (down_grad,) = call(
        functools.partial(down_body, groups=2),
        at,
        (*cot_groups[0], *cot_groups[1], *hiddens),
        [((width, model_width), f32)],
        keep=False,
    )
    for c in range(chunks):
        own = combine(at, picks, cotangent, backs[c], parts[c], share)
        resid_pieces.append(tp_pieces(own))
        (projected,) = call(
            owg_body,
            at,
            (*resid_pieces[c], *norm_args),
            [((sp_count, chan, eighth // chunks), bf16)],
        )
        arrived.append(sp_all(projected))
    resid_grad, norm_grad, own_sums = call(
        functools.partial(mix_body, parts=parts),
        at,
        (*[p for pieces in resid_pieces for p in pieces], out_weight, *norm_args),
        [((tok_rows, model_width), bf16), ((tok_rows, chan), f32), ((2, tok_rows), f32)],
    )
    others = [tp_swap(own_sums, d) for d in (1, 2, 3)]
    out_weight_grad = jnp.concatenate([jnp.sum(a.astype(f32), axis=0) for a in arrived], axis=1)

    taps_count = conv_taps.shape[0]
    all_sums = own_sums + others[0] + others[1] + others[2]
    normed = (conv_out.astype(f32) - row_mean) * row_rstd
    conv_grad = row_rstd * (
        norm_grad
        - (all_sums[0] / channels)[:, None]
        - normed * (all_sums[1] / channels)[:, None]
    )
    next_rows = passed_along(conv_grad[: taps_count - 1], "sp", -1)
    extended = jnp.concatenate([conv_grad, next_rows], axis=0)
    glu_grad = jnp.zeros_like(conv_grad)
    for lag_index in range(taps_count):
        begin = taps_count - 1 - lag_index
        glu_grad = glu_grad + conv_taps[lag_index][None, :] * extended[begin : begin + tok_rows]
    value_grad = (glu_grad * value_scale).astype(bf16)
    gate_in_grad = (glu_grad * gate_scale).astype(bf16)
    return (
        gate_grad[None],
        up_grad[None],
        down_grad[None],
        resid_grad,
        out_weight_grad,
        value_grad,
        gate_in_grad,
    )


def solution(mesh):
    return jax.shard_map(
        on_device,
        mesh=mesh,
        in_specs=(
            P("sp", None),
            P("sp", None),
            P("sp", None),
            P("sp", None),
            P("sp", None, "tp"),
            P("sp", None, "tp"),
            P("sp", "tp", None),
            P("sp", "tp"),
            P("sp", "tp"),
            P("sp", "tp"),
            P(None, "tp"),
            P("tp"),
            P("tp"),
            P("tp", None),
        ),
        out_specs=(
            P("sp", None, "tp"),
            P("sp", None, "tp"),
            P("sp", "tp", None),
            P("sp", None),
            P("tp", "sp"),
            P("sp", "tp"),
            P("sp", "tp"),
        ),
        check_vma=False,
    )
```

time: 438 us -> 254 us (0.58)
  waiting for transfers between devices: 300 us -> 82.8 us
  starting transfers between devices: 19.1 us -> 88 us
  Pallas kernels: 0 us -> 48.5 us
  matrix products: 41.8 us -> 0 us
  blocking collectives: 12.6 us -> 0 us
  between operations: 14.2 us -> 1.77 us
  other arithmetic: 18.6 us -> 9.32 us
  local copies, waits for them, and re-layouts: 30.7 us -> 22.2 us
    all_to_all x3 -> x2, waiting for transfers between devices: 209 us -> 0.01 us  [sp_all(): return lax.all_to_all(value, 'sp', split_axis=0, concat_axis=0, tiled=True)]
    reduce_scatter x2 -> x0, waiting for transfers between devices: 90.5 us -> none  [the longest x1 47 us: on_device(): lax.psum_scatter(partial_low, 'tp', scatter_dimension=2, tiled=True)]
    ppermute x0 -> x60, waiting for transfers between devices: none -> 82.8 us  [the longest x32 45.2 us: tp_swap(): return lax.ppermute(value, 'tp', [(i, i ^ dist) for i in range(count)])]
    ppermute x0 -> x60, starting transfers between devices: none -> 75.5 us  [the longest x28 57.6 us: sp_swap(): return lax.ppermute(value, 'sp', [(i, i ^ dist) for i in range(count)])]
    pallas_call x0 -> x22, Pallas kernels: none -> 48.5 us  [call(): pl.pallas_call(body, grid_spec=pltpu.PrefetchScalarGridSpec(num_scalar_pr...]
    dot_general x10 -> x0, matrix products: 41.8 us -> none  [the longest x1 5.37 us: on_device(): jnp.einsum('lrd,lrf->ldf', slot_rows, gate_pre, preferred_element_type=jn...]
    gather x4 -> x0, local copies, waits for them, and re-layouts: 19.2 us -> none  [the longest x1 6.01 us: on_device(): send_rows = padded_in[token_of].reshape(experts, capacity, model_width)]
    unnamed x38 -> x179, local copies, waits for them, and re-layouts: 3.03 us -> 21.2 us
  transfers between devices with their start and end apart: 7 -> 63, of which waited for: 6 -> 19; matrix products, arithmetic and copies ran while one was open for 12% -> 3% of each run, Pallas kernels for 0% -> 18%
where the time goes in v1:
time: 254 us; the launch traced here: 253 us
  starting transfers between devices  88 us (35%)
  waiting for transfers between devices  82.8 us (33%)
  Pallas kernels  48.5 us (19%)
  local copies, waits for them, and re-layouts  22.2 us (9%)
  other arithmetic  9.32 us (4%)
    ppermute x28, starting transfers between devices, sp_swap(): return lax.ppermute(value, 'sp', [(i, i ^ dist) for i in range(count)])  57.6 us
    pallas_call x22, Pallas kernels, call(): pl.pallas_call(body, grid_spec=pltpu.PrefetchScalarGridSpec(num_scalar_pr...  48.5 us
    ppermute x32, waiting for transfers between devices, tp_swap(): return lax.ppermute(value, 'tp', [(i, i ^ dist) for i in range(count)])  45.2 us
    ppermute x28, waiting for transfers between devices, sp_swap(): return lax.ppermute(value, 'sp', [(i, i ^ dist) for i in range(count)])  37.5 us
    unnamed x179, local copies, waits for them, and re-layouts  21.2 us
    ppermute x32, starting transfers between devices, tp_swap(): return lax.ppermute(value, 'tp', [(i, i ^ dist) for i in range(count)])  17.9 us
    all_to_all x2, starting transfers between devices, sp_all(): return lax.all_to_all(value, 'sp', split_axis=0, concat_axis=0, tiled=True)  11.2 us
  transfers between devices with their start and end apart: 63, of which 19 were waited for; matrix products, arithmetic and copies ran while one was open for 3% of the time, Pallas kernels for 18%

profile of v1, /device:TPU:0, one launch (start us, length us, event | category | flops | bytes accessed | tf_op | source)
XLA Modules:
  0.0 252.6 jit_solution(8636191115212296469)
XLA Ops:
  1.3 3.4 %shard_map.189 = (bf16[144,512]{1,0:T(8,128)(2,1)}, bf16[144,512]{1,0:T(8,128)(2,1)}, bf16[144,512]{1,0:T(8,128)(2,1)}, bf16[144,512]{1,0:T(8,128)(2,1)}, bf16[1...) custom-call(s32[2]{0:T(128)} %pad_add_fusion.at_ref, ...), custom_call_target="tpu_custom_call" | custom-call | tf_op jit(solution)/shard_map/pallas_call | solution.py:87
  4.7 4.1 %collective-permute-start.6 = (bf16[144,512]{1,0:T(8,128)(2,1)}, bf16[144,512]{1,0:T(8,128)(2,1)S(1)}, u32[]{:S(2)}, u32[]{:S(2)}) collective-permute-start(bf16[144,512]{1,0:T(8,128)(2,1)} %get-tuple-element.70), channel_id=1, source_target_pairs={{0,16},{4,20},{8,24},{12,28},{16,0},{20,4},{24,8},{28,12},{1,17},{... | collective-permute-start | bytes 442376 | tf_op jit(solution)/shard_map/ppermute | solution.py:111
  10.1 3.6 %collective-permute-start.8 = (bf16[144,512]{1,0:T(8,128)(2,1)}, bf16[144,512]{1,0:T(8,128)(2,1)S(1)}, u32[]{:S(2)}, u32[]{:S(2)}) collective-permute-start(bf16[144,512]{1,0:T(8,128)(2,1)} %get-tuple-element.72), channel_id=1, source_target_pairs={{0,24},{4,28},{8,16},{12,20},{16,8},{20,12},{24,0},{28,4},{1,25},{... | collective-permute-start | bytes 442376 | tf_op jit(solution)/shard_map/ppermute | solution.py:111
  13.7 1.7 collective-permute-start
  15.4 1.6 shard_map.190
  17.0 9.3 %collective-permute-done.6 = bf16[144,512]{1,0:T(8,128)(2,1)S(1)} collective-permute-done((bf16[144,512]{1,0:T(8,128)(2,1)}, bf16[144,512]{1,0:T(8,128)(2,1)S(1)}, u32[]{:S(2)}, u32[]{:S(2)}) %collective-permute-start.6) | collective-permute-done | bytes 147488 | tf_op jit(solution)/shard_map/ppermute | solution.py:111
  26.4 4.3 %collective-permute-done.7 = bf16[144,512]{1,0:T(8,128)(2,1)S(1)} collective-permute-done((bf16[144,512]{1,0:T(8,128)(2,1)}, bf16[144,512]{1,0:T(8,128)(2,1)S(1)}, u32[]{:S(2)}, u32[]{:S(2)}) %collective-permute-start.7) | collective-permute-done | bytes 147488 | tf_op jit(solution)/shard_map/ppermute | solution.py:111
  30.8 3.8 %collective-permute-start.19 = (bf16[144,512]{1,0:T(8,128)(2,1)S(1)}, bf16[144,512]{1,0:T(8,128)(2,1)S(1)}, u32[]{:S(2)}, u32[]{:S(2)}) collective-permute-start(bf16[144,512]{1,0:T(8,128)(2,1)S(1)} %get-tuple-element.81), channel_id=1, source_target_pairs={{0,16},{4,20},{8,24},{12,28},{16,0},{20,4},{24,8},{28,12},{1,17},{... | collective-permute-start | bytes 442376 | tf_op jit(solution)/shard_map/ppermute | solution.py:111
  36.2 8.5 %collective-permute-start.20 = (bf16[144,512]{1,0:T(8,128)(2,1)S(1)}, bf16[144,512]{1,0:T(8,128)(2,1)S(1)}, u32[]{:S(2)}, u32[]{:S(2)}) collective-permute-start(bf16[144,512]{1,0:T(8,128)(2,1)S(1)} %get-tuple-element.82), channel_id=1, source_target_pairs={{0,20},{4,16},{8,28},{12,24},{16,4},{20,0},{24,12},{28,8},{1,21},{... | collective-permute-start | bytes 442376 | tf_op jit(solution)/shard_map/ppermute | solution.py:111
  45.4 4.2 %collective-permute-start.22 = (bf16[144,512]{1,0:T(8,128)(2,1)S(1)}, bf16[144,512]{1,0:T(8,128)(2,1)S(1)}, u32[]{:S(2)}, u32[]{:S(2)}) collective-permute-start(bf16[144,512]{1,0:T(8,128)(2,1)S(1)} %get-tuple-element.84), channel_id=1, source_target_pairs={{0,28},{4,24},{8,20},{12,16},{16,12},{20,8},{24,4},{28,0},{1,29},{... | collective-permute-start | bytes 442376 | tf_op jit(solution)/shard_map/ppermute | solution.py:111
  49.5 9.3 %collective-permute-done.20 = bf16[144,512]{1,0:T(8,128)(2,1)S(1)} collective-permute-done((bf16[144,512]{1,0:T(8,128)(2,1)S(1)}, bf16[144,512]{1,0:T(8,128)(2,1)S(1)}, u32[]{:S(2)}, u32[]{:S(2)}) %collective-permute-start.20) | collective-permute-done | bytes 147488 | tf_op jit(solution)/shard_map/ppermute | solution.py:111
  60.4 2.3 collective-permute-start.14
  62.7 3.8 %collective-permute-start.15 = (bf16[144,512]{1,0:T(8,128)(2,1)S(1)}, bf16[144,512]{1,0:T(8,128)(2,1)S(1)}, u32[]{:S(2)}, u32[]{:S(2)}) collective-permute-start(bf16[144,512]{1,0:T(8,128)(2,1)S(1)} %get-tuple-element.77), channel_id=1, source_target_pairs={{0,12},{4,8},{8,4},{12,0},{16,28},{20,24},{24,20},{28,16},{1,13},{... | collective-permute-start | bytes 442376 | tf_op jit(solution)/shard_map/ppermute | solution.py:111
  67.5 2.9 %collective-permute-done.15 = bf16[144,512]{1,0:T(8,128)(2,1)S(1)} collective-permute-done((bf16[144,512]{1,0:T(8,128)(2,1)S(1)}, bf16[144,512]{1,0:T(8,128)(2,1)S(1)}, u32[]{:S(2)}, u32[]{:S(2)}) %collective-permute-start.15) | collective-permute-done | bytes 147488 | tf_op jit(solution)/shard_map/ppermute | solution.py:111
  72.6 10.3 %collective-permute-done.24.p2.refs_6_ = bf16[4,144,512]{2,1,0:T(8,128)(2,1)S(1)} collective-permute-done((bf16[4,144,512]{2,1,0:T(8,128)(2,1)S(1)}, bf16[4,144,512]{2,1,0:T(8,128)(2,1)S(1)}, u32[]{:S(2)}, u32[]{:S(2)}) %collective-permute-start.24) | collective-permute-done | bytes 589856 | tf_op jit(solution)/shard_map/ppermute | solution.py:36
  82.9 12.6 %collective-permute-done.4.p2.refs_2_ = bf16[4,144,512]{2,1,0:T(8,128)(2,1)S(1)} collective-permute-done((bf16[4,144,512]{2,1,0:T(8,128)(2,1)S(1)}, bf16[4,144,512]{2,1,0:T(8,128)(2,1)S(1)}, u32[]{:S(2)}, u32[]{:S(2)}) %collective-permute-start.4) | collective-permute-done | bytes 589856 | tf_op jit(solution)/shard_map/ppermute | solution.py:36
  96.0 10.7 %collective-permute-done.17.p2.refs_2_ = bf16[4,144,512]{2,1,0:T(8,128)(2,1)S(1)} collective-permute-done((bf16[4,144,512]{2,1,0:T(8,128)(2,1)S(1)}, bf16[4,144,512]{2,1,0:T(8,128)(2,1)S(1)}, u32[]{:S(2)}, u32[]{:S(2)}) %collective-permute-start.17) | collective-permute-done | bytes 589856 | tf_op jit(solution)/shard_map/ppermute | solution.py:36
  107.3 2.3 shard_map.193
  109.7 1.6 shard_map.194
  112.1 2.0 shard_map.200
  114.9 2.1 shard_map.191
  117.1 1.6 shard_map.192
  119.6 2.0 shard_map.199
  130.9 2.4 collective-permute-done.29.refs_5_
  133.3 6.3 %collective-permute-done.27.refs_2_ = bf16[4,144,256]{2,1,0:T(8,128)(2,1)S(1)} collective-permute-done((bf16[4,144,256]{2,1,0:T(8,128)(2,1)S(1)}, bf16[4,144,256]{2,1,0:T(8,128)(2,1)S(1)}, u32[]{:S(2)}, u32[]{:S(2)}) %collective-permute-start.27) | collective-permute-done | bytes 294944 | tf_op jit(solution)/shard_map/ppermute | solution.py:36
  141.8 2.6 %collective-permute-start.32 = (bf16[144,256]{1,0:T(8,128)(2,1)S(1)}, bf16[144,256]{1,0:T(8,128)(2,1)S(1)}, u32[]{:S(2)}, u32[]{:S(2)}) collective-permute-start(bf16[144,256]{1,0:T(8,128)(2,1)S(1)} %get-tuple-element.101), channel_id=1, source_target_pairs={{0,12},{4,8},{8,4},{12,0},{16,28},{20,24},{24,20},{28,16},{1,13},{... | collective-permute-start | bytes 221192 | tf_op jit(solution)/shard_map/ppermute | solution.py:111
  145.8 2.7 %collective-permute-start.34 = (bf16[144,256]{1,0:T(8,128)(2,1)}, bf16[144,256]{1,0:T(8,128)(2,1)S(1)}, u32[]{:S(2)}, u32[]{:S(2)}) collective-permute-start(bf16[144,256]{1,0:T(8,128)(2,1)} %get-tuple-element.103), channel_id=1, source_target_pairs={{0,20},{4,16},{8,28},{12,24},{16,4},{20,0},{24,12},{28,8},{1,21},{... | collective-permute-start | bytes 221192 | tf_op jit(solution)/shard_map/ppermute | solution.py:111
  149.6 4.2 %collective-permute-done.33.refs_4_ = bf16[144,256]{1,0:T(8,128)(2,1)S(1)} collective-permute-done((bf16[144,256]{1,0:T(8,128)(2,1)S(1)}, bf16[144,256]{1,0:T(8,128)(2,1)S(1)}, u32[]{:S(2)}, u32[]{:S(2)}) %collective-permute-start.33) | collective-permute-done | bytes 73760 | tf_op jit(solution)/shard_map/ppermute | solution.py:111
  153.8 3.5 %collective-permute-start.36 = (bf16[144,256]{1,0:T(8,128)(2,1)}, bf16[144,256]{1,0:T(8,128)(2,1)}, u32[]{:S(2)}, u32[]{:S(2)}) collective-permute-start(bf16[144,256]{1,0:T(8,128)(2,1)} %get-tuple-element.105), channel_id=1, source_target_pairs={{0,28},{4,24},{8,20},{12,16},{16,12},{20,8},{24,4},{28,0},{1,29},{... | collective-permute-start | bytes 221192 | tf_op jit(solution)/shard_map/ppermute | solution.py:111
  163.0 2.0 shard_map.202.refs_0_.p0
  165.9 1.8 shard_map.203
  168.8 2.5 collective-permute-start.46
  172.7 1.9 collective-permute-start.48
  174.6 2.3 collective-permute-start.49
  176.9 1.9 collective-permute-start.50
  178.9 2.0 collective-permute-done.49.refs_6_
  180.9 3.1 %collective-permute-done.50.refs_7_ = bf16[144,256]{1,0:T(8,128)(2,1)S(1)} collective-permute-done((bf16[144,256]{1,0:T(8,128)(2,1)S(1)}, bf16[144,256]{1,0:T(8,128)(2,1)S(1)}, u32[]{:S(2)}, u32[]{:S(2)}) %collective-permute-start.50) | collective-permute-done | bytes 73760 | tf_op jit(solution)/shard_map/ppermute | solution.py:111
  185.1 2.1 collective-permute-start.52
  188.9 1.7 collective-permute-start.55
  194.7 2.0 shard_map.208
  196.7 4.4 %all-to-all-start = ((bf16[8,256,128]{2,1,0:T(8,128)(2,1)}), bf16[8,256,128]{2,1,0:T(8,128)(2,1)}, u32[]{:S(2)}, u32[]{:S(2)}) async-start(bf16[8,256,128]{2,1,0:T(8,128)(2,1)} %shard_map.208), calls=%async_computation | async-start | bytes 1048576 | tf_op jit(solution)/shard_map/all_to_all | solution.py:122
  207.5 4.2 %shard_map.207 = (bf16[384,2048]{1,0:T(8,128)(2,1)}, f32[384,256]{1,0:T(8,128)S(1)}, f32[2,384]{1,0:T(2,128)S(1)}) custom-call(s32[2]{0:T(128)S(1)} %copy-done.54, bf16[384,256]{1,0:T(8,128)(2,1)S(1)} %shard_map.202.refs_0_.p0, bf16[384,256]{1,0:T(8,128)(2,1)S(1)} %copy-done.43, bf16[384,256]{1,0:T(8,128)(2,1)S(1)} %collective-permute-done.38.refs_2_.p2, ...), custom_call_target="tpu_custom_call" | custom-call | tf_op jit(solution)/shard_map/pallas_call | solution.py:87
  213.8 2.2 shard_map.209
  219.1 6.9 %all-to-all-start.1 = ((bf16[8,256,128]{2,1,0:T(8,128)(2,1)}), bf16[8,256,128]{2,1,0:T(8,128)(2,1)}, u32[]{:S(2)}, u32[]{:S(2)}) async-start(bf16[8,256,128]{2,1,0:T(8,128)(2,1)} %copy-done.25), calls=%async_computation.1 | async-start | bytes 1048576 | tf_op jit(solution)/shard_map/all_to_all | solution.py:122
  232.8 3.5 %shard_map.195 = f32[2048,256]{1,0:T(8,128)} custom-call(s32[2]{0:T(128)S(1)} %copy-done.54, bf16[4,144,512]{2,1,0:T(8,128)(2,1)S(1)} %pad_maximum_fusion.p0.refs_0_, bf16[4,144,512]{2,1,0:T(8,128)(2,1)S(1)} %copy-done.14, bf16[4,144,512]{2,1,0:T(8,128)(2,1)S(1)} %copy-done.10, bf16[4,144,512]{2,1,0:T(8,128)(2,1)S(1)} %copy-done.16, ...), custom_call_target="tpu_custom_call" | custom-call | tf_op jit(solution)/shard_map/pallas_call | solution.py:87
  236.3 3.5 %shard_map.196 = f32[2048,256]{1,0:T(8,128)} custom-call(s32[2]{0:T(128)S(1)} %copy-done.54, bf16[4,144,512]{2,1,0:T(8,128)(2,1)S(1)} %pad_maximum_fusion.p0.refs_0_, bf16[4,144,512]{2,1,0:T(8,128)(2,1)S(1)} %copy-done.14, bf16[4,144,512]{2,1,0:T(8,128)(2,1)S(1)} %copy-done.10, bf16[4,144,512]{2,1,0:T(8,128)(2,1)S(1)} %copy-done.16, ...), custom_call_target="tpu_custom_call" | custom-call | tf_op jit(solution)/shard_map/pallas_call | solution.py:87
  239.9 6.1 %shard_map.197 = f32[256,2048]{1,0:T(8,128)} custom-call(s32[2]{0:T(128)} %pad_add_fusion.at_ref, bf16[4,144,512]{2,1,0:T(8,128)(2,1)} %copy-done.4, bf16[4,144,512]{2,1,0:T(8,128)(2,1)} %copy-done.23, bf16[4,144,512]{2,1,0:T(8,128)(2,1)} %copy-done.21, bf16[4,144,512]{2,1,0:T(8,128)(2,1)} %copy-done.24, bf16[4,144,512]{2,1,0:T(8,128)(2,1)} %copy-done.3, ...), custom_call_target="tpu_custom_call" | custom-call | tf_op jit(solution)/shard_map/pallas_call | solution.py:87
  246.2 2.6 %multiply_convert_fusion = (bf16[384,256]{1,0:T(8,128)(2,1)}, f32[384,256]{1,0:T(8,128)S(1)}) fusion(f32[384,256]{1,0:T(8,128)S(1)} %get-tuple-element.124, f32[384,256]{1,0:T(8,128)S(1)} %copy-done.66, f32[256]{0:T(256)S(1)} %bitcast.127, f32[30,256]{1,0:T(8,128)S(1)} %collective-permute-done.60, f32[256]{0:T(256)S(1)} %bitcast.128, f32[256]{0:T(256)S(1)} %bitcast.99, ...), kind=kLoop, calls=%fused_computation.154 | loop fusion | flops 9142272 | bytes 1438720 | tf_op jit(solution)/shard_map/convert_element_type | solution.py:497
  (300 shorter events, 64.4 us)
Async XLA Ops:
  4.7 21.7 %collective-permute-start.6 = (bf16[144,512]{1,0:T(8,128)(2,1)}, bf16[144,512]{1,0:T(8,128)(2,1)S(1)}, u32[]{:S(2)}, u32[]{:S(2)}) collective-permute-start(bf16[144,512]{1,0:T(8,128)(2,1)} %get-tuple-element.70), channel_id=1, source_target_pairs={{0,16},{4,20},{8,24},{12,28},{16,0},{20,4},{24,8},{28,12},{1,17},{... | collective-permute-start | bytes 442376 | tf_op jit(solution)/shard_map/ppermute | solution.py:111
  8.8 22.0 %collective-permute-start.7 = (bf16[144,512]{1,0:T(8,128)(2,1)}, bf16[144,512]{1,0:T(8,128)(2,1)S(1)}, u32[]{:S(2)}, u32[]{:S(2)}) collective-permute-start(bf16[144,512]{1,0:T(8,128)(2,1)} %get-tuple-element.71), channel_id=1, source_target_pairs={{0,20},{4,16},{8,28},{12,24},{16,4},{20,0},{24,12},{28,8},{1,21},{... | collective-permute-start | bytes 442376 | tf_op jit(solution)/shard_map/ppermute | solution.py:111
  10.1 20.7 %collective-permute-start.8 = (bf16[144,512]{1,0:T(8,128)(2,1)}, bf16[144,512]{1,0:T(8,128)(2,1)S(1)}, u32[]{:S(2)}, u32[]{:S(2)}) collective-permute-start(bf16[144,512]{1,0:T(8,128)(2,1)} %get-tuple-element.72), channel_id=1, source_target_pairs={{0,24},{4,28},{8,16},{12,20},{16,8},{20,12},{24,0},{28,4},{1,25},{... | collective-permute-start | bytes 442376 | tf_op jit(solution)/shard_map/ppermute | solution.py:111
  13.7 20.9 %collective-permute-start.9 = (bf16[144,512]{1,0:T(8,128)(2,1)}, bf16[144,512]{1,0:T(8,128)(2,1)S(1)}, u32[]{:S(2)}, u32[]{:S(2)}) collective-permute-start(bf16[144,512]{1,0:T(8,128)(2,1)} %get-tuple-element.73), channel_id=1, source_target_pairs={{0,28},{4,24},{8,20},{12,16},{16,12},{20,8},{24,4},{28,0},{1,29},{... | collective-permute-start | bytes 442376 | tf_op jit(solution)/shard_map/ppermute | solution.py:111
  13.7 22.5 %collective-permute-start = (bf16[144,512]{1,0:T(8,128)(2,1)}, bf16[144,512]{1,0:T(8,128)(2,1)S(1)}, u32[]{:S(2)}, u32[]{:S(2)}) collective-permute-start(bf16[144,512]{1,0:T(8,128)(2,1)} %get-tuple-element.67), channel_id=1, source_target_pairs={{0,4},{4,0},{8,12},{12,8},{16,20},{20,16},{24,28},{28,24},{1,5},{5... | collective-permute-start | bytes 442376 | tf_op jit(solution)/shard_map/ppermute | solution.py:111
  26.4 9.8 %collective-permute-start.1 = (bf16[144,512]{1,0:T(8,128)(2,1)S(1)}, bf16[144,512]{1,0:T(8,128)(2,1)S(1)}, u32[]{:S(2)}, u32[]{:S(2)}) collective-permute-start(bf16[144,512]{1,0:T(8,128)(2,1)S(1)} %copy-done.88), channel_id=1, source_target_pairs={{0,8},{4,12},{8,0},{12,4},{16,24},{20,28},{24,16},{28,20},{1,9},{5... | collective-permute-start | bytes 442376 | tf_op jit(solution)/shard_map/ppermute | solution.py:111
  30.8 13.9 %collective-permute-start.2 = (bf16[144,512]{1,0:T(8,128)(2,1)S(1)}, bf16[144,512]{1,0:T(8,128)(2,1)S(1)}, u32[]{:S(2)}, u32[]{:S(2)}) collective-permute-start(bf16[144,512]{1,0:T(8,128)(2,1)S(1)} %copy-done.87), channel_id=1, source_target_pairs={{0,12},{4,8},{8,4},{12,0},{16,28},{20,24},{24,20},{28,16},{1,13},{... | collective-permute-start | bytes 442376 | tf_op jit(solution)/shard_map/ppermute | solution.py:111
  30.8 14.6 %collective-permute-start.19 = (bf16[144,512]{1,0:T(8,128)(2,1)S(1)}, bf16[144,512]{1,0:T(8,128)(2,1)S(1)}, u32[]{:S(2)}, u32[]{:S(2)}) collective-permute-start(bf16[144,512]{1,0:T(8,128)(2,1)S(1)} %get-tuple-element.81), channel_id=1, source_target_pairs={{0,16},{4,20},{8,24},{12,28},{16,0},{20,4},{24,8},{28,12},{1,17},{... | collective-permute-start | bytes 442376 | tf_op jit(solution)/shard_map/ppermute | solution.py:111
  34.6 36.4 %collective-permute-start.11 = (bf16[4,144,512]{2,1,0:T(8,128)(2,1)S(1)}, bf16[4,144,512]{2,1,0:T(8,128)(2,1)S(1)}, u32[]{:S(2)}, u32[]{:S(2)}) collective-permute-start(bf16[4,144,512]{2,1,0:T(8,128)(2,1)S(1)} %pad_maximum_fusion.1.p0.refs_4_), channel_id=1, source_target_pairs={{0,2},{1,3},{2,0},{3,1},{4,6},{5,7},{6,4},{7,5},{8,10},{9,11},{10,... | collective-permute-start | bytes 1769480 | tf_op jit(solution)/shard_map/ppermute | solution.py:36
  36.2 36.4 %collective-permute-start.10 = (bf16[4,144,512]{2,1,0:T(8,128)(2,1)S(1)}, bf16[4,144,512]{2,1,0:T(8,128)(2,1)S(1)}, u32[]{:S(2)}, u32[]{:S(2)}) collective-permute-start(bf16[4,144,512]{2,1,0:T(8,128)(2,1)S(1)} %pad_maximum_fusion.1.p0.refs_4_), channel_id=1, source_target_pairs={{0,1},{1,0},{2,3},{3,2},{4,5},{5,4},{6,7},{7,6},{8,9},{9,8},{10,11... | collective-permute-start | bytes 1769480 | tf_op jit(solution)/shard_map/ppermute | solution.py:36
  36.2 22.7 %collective-permute-start.20 = (bf16[144,512]{1,0:T(8,128)(2,1)S(1)}, bf16[144,512]{1,0:T(8,128)(2,1)S(1)}, u32[]{:S(2)}, u32[]{:S(2)}) collective-permute-start(bf16[144,512]{1,0:T(8,128)(2,1)S(1)} %get-tuple-element.82), channel_id=1, source_target_pairs={{0,20},{4,16},{8,28},{12,24},{16,4},{20,0},{24,12},{28,8},{1,21},{... | collective-permute-start | bytes 442376 | tf_op jit(solution)/shard_map/ppermute | solution.py:111
  44.7 15.7 %collective-permute-start.21 = (bf16[144,512]{1,0:T(8,128)(2,1)S(1)}, bf16[144,512]{1,0:T(8,128)(2,1)S(1)}, u32[]{:S(2)}, u32[]{:S(2)}) collective-permute-start(bf16[144,512]{1,0:T(8,128)(2,1)S(1)} %get-tuple-element.83), channel_id=1, source_target_pairs={{0,24},{4,28},{8,16},{12,20},{16,8},{20,12},{24,0},{28,4},{1,25},{... | collective-permute-start | bytes 442376 | tf_op jit(solution)/shard_map/ppermute | solution.py:111
  45.4 17.3 %collective-permute-start.22 = (bf16[144,512]{1,0:T(8,128)(2,1)S(1)}, bf16[144,512]{1,0:T(8,128)(2,1)S(1)}, u32[]{:S(2)}, u32[]{:S(2)}) collective-permute-start(bf16[144,512]{1,0:T(8,128)(2,1)S(1)} %get-tuple-element.84), channel_id=1, source_target_pairs={{0,28},{4,24},{8,20},{12,16},{16,12},{20,8},{24,4},{28,0},{1,29},{... | collective-permute-start | bytes 442376 | tf_op jit(solution)/shard_map/ppermute | solution.py:111
  58.9 7.7 %collective-permute-start.13 = (bf16[144,512]{1,0:T(8,128)(2,1)S(1)}, bf16[144,512]{1,0:T(8,128)(2,1)S(1)}, u32[]{:S(2)}, u32[]{:S(2)}) collective-permute-start(bf16[144,512]{1,0:T(8,128)(2,1)S(1)} %get-tuple-element.75), channel_id=1, source_target_pairs={{0,4},{4,0},{8,12},{12,8},{16,20},{20,16},{24,28},{28,24},{1,5},{5... | collective-permute-start | bytes 442376 | tf_op jit(solution)/shard_map/ppermute | solution.py:111
  60.4 7.0 %collective-permute-start.14 = (bf16[144,512]{1,0:T(8,128)(2,1)S(1)}, bf16[144,512]{1,0:T(8,128)(2,1)S(1)}, u32[]{:S(2)}, u32[]{:S(2)}) collective-permute-start(bf16[144,512]{1,0:T(8,128)(2,1)S(1)} %get-tuple-element.76), channel_id=1, source_target_pairs={{0,8},{4,12},{8,0},{12,4},{16,24},{20,28},{24,16},{28,20},{1,9},{5... | collective-permute-start | bytes 442376 | tf_op jit(solution)/shard_map/ppermute | solution.py:111
  62.7 7.7 %collective-permute-start.15 = (bf16[144,512]{1,0:T(8,128)(2,1)S(1)}, bf16[144,512]{1,0:T(8,128)(2,1)S(1)}, u32[]{:S(2)}, u32[]{:S(2)}) collective-permute-start(bf16[144,512]{1,0:T(8,128)(2,1)S(1)} %get-tuple-element.77), channel_id=1, source_target_pairs={{0,12},{4,8},{8,4},{12,0},{16,28},{20,24},{24,20},{28,16},{1,13},{... | collective-permute-start | bytes 442376 | tf_op jit(solution)/shard_map/ppermute | solution.py:111
  66.6 16.3 %collective-permute-start.24 = (bf16[4,144,512]{2,1,0:T(8,128)(2,1)S(1)}, bf16[4,144,512]{2,1,0:T(8,128)(2,1)S(1)}, u32[]{:S(2)}, u32[]{:S(2)}) collective-permute-start(bf16[4,144,512]{2,1,0:T(8,128)(2,1)S(1)} %pad_maximum_fusion.3.p0.refs_4_), channel_id=1, source_target_pairs={{0,2},{1,3},{2,0},{3,1},{4,6},{5,7},{6,4},{7,5},{8,10},{9,11},{10,... | collective-permute-start | bytes 1769480 | tf_op jit(solution)/shard_map/ppermute | solution.py:36
  67.4 28.1 %collective-permute-start.23 = (bf16[4,144,512]{2,1,0:T(8,128)(2,1)S(1)}, bf16[4,144,512]{2,1,0:T(8,128)(2,1)S(1)}, u32[]{:S(2)}, u32[]{:S(2)}) collective-permute-start(bf16[4,144,512]{2,1,0:T(8,128)(2,1)S(1)} %pad_maximum_fusion.3.p0.refs_4_), channel_id=1, source_target_pairs={{0,1},{1,0},{2,3},{3,2},{4,5},{5,4},{6,7},{7,6},{8,9},{9,8},{10,11... | collective-permute-start | bytes 1769480 | tf_op jit(solution)/shard_map/ppermute | solution.py:36
  70.4 25.1 %collective-permute-start.4 = (bf16[4,144,512]{2,1,0:T(8,128)(2,1)S(1)}, bf16[4,144,512]{2,1,0:T(8,128)(2,1)S(1)}, u32[]{:S(2)}, u32[]{:S(2)}) collective-permute-start(bf16[4,144,512]{2,1,0:T(8,128)(2,1)S(1)} %pad_maximum_fusion.p0.refs_0_), channel_id=1, source_target_pairs={{0,2},{1,3},{2,0},{3,1},{4,6},{5,7},{6,4},{7,5},{8,10},{9,11},{10,... | collective-permute-start | bytes 1769480 | tf_op jit(solution)/shard_map/ppermute | solution.py:36
  71.1 35.7 %collective-permute-start.17 = (bf16[4,144,512]{2,1,0:T(8,128)(2,1)S(1)}, bf16[4,144,512]{2,1,0:T(8,128)(2,1)S(1)}, u32[]{:S(2)}, u32[]{:S(2)}) collective-permute-start(bf16[4,144,512]{2,1,0:T(8,128)(2,1)S(1)} %pad_maximum_fusion.2.p0.refs_0_), channel_id=1, source_target_pairs={{0,2},{1,3},{2,0},{3,1},{4,6},{5,7},{6,4},{7,5},{8,10},{9,11},{10,... | collective-permute-start | bytes 1769480 | tf_op jit(solution)/shard_map/ppermute | solution.py:36
  72.6 34.2 %collective-permute-start.12 = (bf16[4,144,512]{2,1,0:T(8,128)(2,1)S(1)}, bf16[4,144,512]{2,1,0:T(8,128)(2,1)S(1)}, u32[]{:S(2)}, u32[]{:S(2)}) collective-permute-start(bf16[4,144,512]{2,1,0:T(8,128)(2,1)S(1)} %collective-permute-done.11.p2.refs_6_), channel_id=1, source_target_pairs={{0,1},{1,0},{2,3},{3,2},{4,5},{5,4},{6,7},{7,6},{8,9},{9,8},{10,11... | collective-permute-start | bytes 1769480 | tf_op jit(solution)/shard_map/ppermute | solution.py:36
  82.9 26.8 %collective-permute-start.25 = (bf16[4,144,512]{2,1,0:T(8,128)(2,1)S(1)}, bf16[4,144,512]{2,1,0:T(8,128)(2,1)S(1)}, u32[]{:S(2)}, u32[]{:S(2)}) collective-permute-start(bf16[4,144,512]{2,1,0:T(8,128)(2,1)S(1)} %collective-permute-done.24.p2.refs_6_), channel_id=1, source_target_pairs={{0,1},{1,0},{2,3},{3,2},{4,5},{5,4},{6,7},{7,6},{8,9},{9,8},{10,11... | collective-permute-start | bytes 1769480 | tf_op jit(solution)/shard_map/ppermute | solution.py:36
  95.5 19.3 %collective-permute-start.3 = (bf16[4,144,512]{2,1,0:T(8,128)(2,1)S(1)}, bf16[4,144,512]{2,1,0:T(8,128)(2,1)S(1)}, u32[]{:S(2)}, u32[]{:S(2)}) collective-permute-start(bf16[4,144,512]{2,1,0:T(8,128)(2,1)S(1)} %pad_maximum_fusion.p0.refs_0_), channel_id=1, source_target_pairs={{0,1},{1,0},{2,3},{3,2},{4,5},{5,4},{6,7},{7,6},{8,9},{9,8},{10,11... | collective-permute-start | bytes 1769480 | tf_op jit(solution)/shard_map/ppermute | solution.py:36
  95.5 19.3 %collective-permute-start.5 = (bf16[4,144,512]{2,1,0:T(8,128)(2,1)S(1)}, bf16[4,144,512]{2,1,0:T(8,128)(2,1)S(1)}, u32[]{:S(2)}, u32[]{:S(2)}) collective-permute-start(bf16[4,144,512]{2,1,0:T(8,128)(2,1)S(1)} %collective-permute-done.4.p2.refs_2_), channel_id=1, source_target_pairs={{0,1},{1,0},{2,3},{3,2},{4,5},{5,4},{6,7},{7,6},{8,9},{9,8},{10,11... | collective-permute-start | bytes 1769480 | tf_op jit(solution)/shard_map/ppermute | solution.py:36
  106.8 10.3 %collective-permute-start.16 = (bf16[4,144,512]{2,1,0:T(8,128)(2,1)S(1)}, bf16[4,144,512]{2,1,0:T(8,128)(2,1)S(1)}, u32[]{:S(2)}, u32[]{:S(2)}) collective-permute-start(bf16[4,144,512]{2,1,0:T(8,128)(2,1)S(1)} %pad_maximum_fusion.2.p0.refs_0_), channel_id=1, source_target_pairs={{0,1},{1,0},{2,3},{3,2},{4,5},{5,4},{6,7},{7,6},{8,9},{9,8},{10,11... | collective-permute-start | bytes 1769480 | tf_op jit(solution)/shard_map/ppermute | solution.py:36
  106.8 10.3 %collective-permute-start.18 = (bf16[4,144,512]{2,1,0:T(8,128)(2,1)S(1)}, bf16[4,144,512]{2,1,0:T(8,128)(2,1)S(1)}, u32[]{:S(2)}, u32[]{:S(2)}) collective-permute-start(bf16[4,144,512]{2,1,0:T(8,128)(2,1)S(1)} %collective-permute-done.17.p2.refs_2_), channel_id=1, source_target_pairs={{0,1},{1,0},{2,3},{3,2},{4,5},{5,4},{6,7},{7,6},{8,9},{9,8},{10,11... | collective-permute-start | bytes 1769480 | tf_op jit(solution)/shard_map/ppermute | solution.py:36
  114.8 8.5 %collective-permute-start.28 = (bf16[8,144,256]{2,1,0:T(8,128)(2,1)S(1)}, bf16[8,144,256]{2,1,0:T(8,128)(2,1)S(1)}, u32[]{:S(2)}, u32[]{:S(2)}) collective-permute-start(bf16[8,144,256]{2,1,0:T(8,128)(2,1)S(1)} %get-tuple-element.96), channel_id=1, source_target_pairs={{0,1},{1,0},{2,3},{3,2},{4,5},{5,4},{6,7},{7,6},{8,9},{9,8},{10,11... | collective-permute-start | bytes 1769480 | tf_op jit(solution)/shard_map/ppermute | solution.py:36
  123.4 9.9 %collective-permute-start.29 = (bf16[4,144,256]{2,1,0:T(8,128)(2,1)S(1)}, bf16[4,144,256]{2,1,0:T(8,128)(2,1)S(1)}, u32[]{:S(2)}, u32[]{:S(2)}) collective-permute-start(bf16[4,144,256]{2,1,0:T(8,128)(2,1)S(1)} %add_convert_fusion.2), channel_id=1, source_target_pairs={{0,2},{1,3},{2,0},{3,1},{4,6},{5,7},{6,4},{7,5},{8,10},{9,11},{10,... | collective-permute-start | bytes 884744 | tf_op jit(solution)/shard_map/ppermute | solution.py:36
  124.4 15.2 %collective-permute-start.27 = (bf16[4,144,256]{2,1,0:T(8,128)(2,1)S(1)}, bf16[4,144,256]{2,1,0:T(8,128)(2,1)S(1)}, u32[]{:S(2)}, u32[]{:S(2)}) collective-permute-start(bf16[4,144,256]{2,1,0:T(8,128)(2,1)S(1)} %add_convert_fusion.3), channel_id=1, source_target_pairs={{0,2},{1,3},{2,0},{3,1},{4,6},{5,7},{6,4},{7,5},{8,10},{9,11},{10,... | collective-permute-start | bytes 884744 | tf_op jit(solution)/shard_map/ppermute | solution.py:36
  127.3 38.6 %collective-permute-start.43 = (bf16[4,144,256]{2,1,0:T(8,128)(2,1)}, bf16[4,144,256]{2,1,0:T(8,128)(2,1)}, u32[]{:S(2)}, u32[]{:S(2)}) collective-permute-start(bf16[4,144,256]{2,1,0:T(8,128)(2,1)} %add_convert_fusion), channel_id=1, source_target_pairs={{0,2},{1,3},{2,0},{3,1},{4,6},{5,7},{6,4},{7,5},{8,10},{9,11},{10,... | collective-permute-start | bytes 884744 | tf_op jit(solution)/shard_map/ppermute | solution.py:36
  129.8 36.0 %collective-permute-start.41 = (bf16[4,144,256]{2,1,0:T(8,128)(2,1)}, bf16[4,144,256]{2,1,0:T(8,128)(2,1)}, u32[]{:S(2)}, u32[]{:S(2)}) collective-permute-start(bf16[4,144,256]{2,1,0:T(8,128)(2,1)} %add_convert_fusion.1), channel_id=1, source_target_pairs={{0,2},{1,3},{2,0},{3,1},{4,6},{5,7},{6,4},{7,5},{8,10},{9,11},{10,... | collective-permute-start | bytes 884744 | tf_op jit(solution)/shard_map/ppermute | solution.py:36
  141.8 6.9 %collective-permute-start.32 = (bf16[144,256]{1,0:T(8,128)(2,1)S(1)}, bf16[144,256]{1,0:T(8,128)(2,1)S(1)}, u32[]{:S(2)}, u32[]{:S(2)}) collective-permute-start(bf16[144,256]{1,0:T(8,128)(2,1)S(1)} %get-tuple-element.101), channel_id=1, source_target_pairs={{0,12},{4,8},{8,4},{12,0},{16,28},{20,24},{24,20},{28,16},{1,13},{... | collective-permute-start | bytes 221192 | tf_op jit(solution)/shard_map/ppermute | solution.py:111
  145.4 8.4 %collective-permute-start.33 = (bf16[144,256]{1,0:T(8,128)(2,1)S(1)}, bf16[144,256]{1,0:T(8,128)(2,1)S(1)}, u32[]{:S(2)}, u32[]{:S(2)}) collective-permute-start(bf16[144,256]{1,0:T(8,128)(2,1)S(1)} %get-tuple-element.102), channel_id=1, source_target_pairs={{0,16},{4,20},{8,24},{12,28},{16,0},{20,4},{24,8},{28,12},{1,17},{... | collective-permute-start | bytes 221192 | tf_op jit(solution)/shard_map/ppermute | solution.py:111
  145.8 13.1 %collective-permute-start.34 = (bf16[144,256]{1,0:T(8,128)(2,1)}, bf16[144,256]{1,0:T(8,128)(2,1)S(1)}, u32[]{:S(2)}, u32[]{:S(2)}) collective-permute-start(bf16[144,256]{1,0:T(8,128)(2,1)} %get-tuple-element.103), channel_id=1, source_target_pairs={{0,20},{4,16},{8,28},{12,24},{16,4},{20,0},{24,12},{28,8},{1,21},{... | collective-permute-start | bytes 221192 | tf_op jit(solution)/shard_map/ppermute | solution.py:111
  148.7 10.8 %collective-permute-start.35 = (bf16[144,256]{1,0:T(8,128)(2,1)}, bf16[144,256]{1,0:T(8,128)(2,1)S(1)}, u32[]{:S(2)}, u32[]{:S(2)}) collective-permute-start(bf16[144,256]{1,0:T(8,128)(2,1)} %get-tuple-element.104), channel_id=1, source_target_pairs={{0,24},{4,28},{8,16},{12,20},{16,8},{20,12},{24,0},{28,4},{1,25},{... | collective-permute-start | bytes 221192 | tf_op jit(solution)/shard_map/ppermute | solution.py:111
  153.8 7.4 %collective-permute-start.36 = (bf16[144,256]{1,0:T(8,128)(2,1)}, bf16[144,256]{1,0:T(8,128)(2,1)}, u32[]{:S(2)}, u32[]{:S(2)}) collective-permute-start(bf16[144,256]{1,0:T(8,128)(2,1)} %get-tuple-element.105), channel_id=1, source_target_pairs={{0,28},{4,24},{8,20},{12,16},{16,12},{20,8},{24,4},{28,0},{1,29},{... | collective-permute-start | bytes 221192 | tf_op jit(solution)/shard_map/ppermute | solution.py:111
  165.0 22.2 %collective-permute-start.38 = (bf16[384,256]{1,0:T(8,128)(2,1)S(1)}, bf16[384,256]{1,0:T(8,128)(2,1)S(1)}, u32[]{:S(2)}, u32[]{:S(2)}) collective-permute-start(bf16[384,256]{1,0:T(8,128)(2,1)S(1)} %shard_map.202.refs_0_.p0), channel_id=1, source_target_pairs={{0,2},{1,3},{2,0},{3,1},{4,6},{5,7},{6,4},{7,5},{8,10},{9,11},{10,... | collective-permute-start | bytes 589832 | tf_op jit(solution)/shard_map/ppermute | solution.py:36
  168.8 8.2 %collective-permute-start.46 = (bf16[144,256]{1,0:T(8,128)(2,1)S(1)}, bf16[144,256]{1,0:T(8,128)(2,1)S(1)}, u32[]{:S(2)}, u32[]{:S(2)}) collective-permute-start(bf16[144,256]{1,0:T(8,128)(2,1)S(1)} %get-tuple-element.115), channel_id=1, source_target_pairs={{0,12},{4,8},{8,4},{12,0},{16,28},{20,24},{24,20},{28,16},{1,13},{... | collective-permute-start | bytes 221192 | tf_op jit(solution)/shard_map/ppermute | solution.py:111
  171.2 7.7 %collective-permute-start.47 = (bf16[144,256]{1,0:T(8,128)(2,1)S(1)}, bf16[144,256]{1,0:T(8,128)(2,1)S(1)}, u32[]{:S(2)}, u32[]{:S(2)}) collective-permute-start(bf16[144,256]{1,0:T(8,128)(2,1)S(1)} %get-tuple-element.116), channel_id=1, source_target_pairs={{0,16},{4,20},{8,24},{12,28},{16,0},{20,4},{24,8},{28,12},{1,17},{... | collective-permute-start | bytes 221192 | tf_op jit(solution)/shard_map/ppermute | solution.py:111
  176.9 7.1 %collective-permute-start.50 = (bf16[144,256]{1,0:T(8,128)(2,1)S(1)}, bf16[144,256]{1,0:T(8,128)(2,1)S(1)}, u32[]{:S(2)}, u32[]{:S(2)}) collective-permute-start(bf16[144,256]{1,0:T(8,128)(2,1)S(1)} %get-tuple-element.119), channel_id=1, source_target_pairs={{0,28},{4,24},{8,20},{12,16},{16,12},{20,8},{24,4},{28,0},{1,29},{... | collective-permute-start | bytes 221192 | tf_op jit(solution)/shard_map/ppermute | solution.py:111
  185.1 9.2 %collective-permute-start.52 = (bf16[384,256]{1,0:T(8,128)(2,1)S(1)}, bf16[384,256]{1,0:T(8,128)(2,1)S(1)}, u32[]{:S(2)}, u32[]{:S(2)}) collective-permute-start(bf16[384,256]{1,0:T(8,128)(2,1)S(1)} %shard_map.204.refs_4_.p0), channel_id=1, source_target_pairs={{0,2},{1,3},{2,0},{3,1},{4,6},{5,7},{6,4},{7,5},{8,10},{9,11},{10,... | collective-permute-start | bytes 589832 | tf_op jit(solution)/shard_map/ppermute | solution.py:36
  187.2 7.5 %collective-permute-start.37 = (bf16[384,256]{1,0:T(8,128)(2,1)S(1)}, bf16[384,256]{1,0:T(8,128)(2,1)S(1)}, u32[]{:S(2)}, u32[]{:S(2)}) collective-permute-start(bf16[384,256]{1,0:T(8,128)(2,1)S(1)} %shard_map.202.refs_0_.p0), channel_id=1, source_target_pairs={{0,1},{1,0},{2,3},{3,2},{4,5},{5,4},{6,7},{7,6},{8,9},{9,8},{10,11... | collective-permute-start | bytes 589832 | tf_op jit(solution)/shard_map/ppermute | solution.py:36
  187.2 7.5 %collective-permute-start.39 = (bf16[384,256]{1,0:T(8,128)(2,1)S(1)}, bf16[384,256]{1,0:T(8,128)(2,1)S(1)}, u32[]{:S(2)}, u32[]{:S(2)}) collective-permute-start(bf16[384,256]{1,0:T(8,128)(2,1)S(1)} %collective-permute-done.38.refs_2_.p2), channel_id=1, source_target_pairs={{0,1},{1,0},{2,3},{3,2},{4,5},{5,4},{6,7},{7,6},{8,9},{9,8},{10,11... | collective-permute-start | bytes 589832 | tf_op jit(solution)/shard_map/ppermute | solution.py:36
  194.1 7.7 %collective-permute-start.51 = (bf16[384,256]{1,0:T(8,128)(2,1)S(1)}, bf16[384,256]{1,0:T(8,128)(2,1)S(1)}, u32[]{:S(2)}, u32[]{:S(2)}) collective-permute-start(bf16[384,256]{1,0:T(8,128)(2,1)S(1)} %shard_map.204.refs_4_.p0), channel_id=1, source_target_pairs={{0,1},{1,0},{2,3},{3,2},{4,5},{5,4},{6,7},{7,6},{8,9},{9,8},{10,11... | collective-permute-start | bytes 589832 | tf_op jit(solution)/shard_map/ppermute | solution.py:36
  194.3 8.2 %collective-permute-start.53 = (bf16[384,256]{1,0:T(8,128)(2,1)S(1)}, bf16[384,256]{1,0:T(8,128)(2,1)}, u32[]{:S(2)}, u32[]{:S(2)}) collective-permute-start(bf16[384,256]{1,0:T(8,128)(2,1)S(1)} %collective-permute-done.52.refs_6_.p2), channel_id=1, source_target_pairs={{0,1},{1,0},{2,3},{3,2},{4,5},{5,4},{6,7},{7,6},{8,9},{9,8},{10,11... | collective-permute-start | bytes 589832 | tf_op jit(solution)/shard_map/ppermute | solution.py:36
  196.7 22.4 %all-to-all-start = ((bf16[8,256,128]{2,1,0:T(8,128)(2,1)}), bf16[8,256,128]{2,1,0:T(8,128)(2,1)}, u32[]{:S(2)}, u32[]{:S(2)}) async-start(bf16[8,256,128]{2,1,0:T(8,128)(2,1)} %shard_map.208), calls=%async_computation | async-start | bytes 1048576 | tf_op jit(solution)/shard_map/all_to_all | solution.py:122
  217.8 28.2 %collective-permute-start.60 = (f32[30,256]{1,0:T(8,128)S(1)}, f32[30,256]{1,0:T(8,128)S(1)}, u32[]{:S(2)}, u32[]{:S(2)}) collective-permute-start(f32[30,256]{1,0:T(8,128)S(1)} %slice.288), channel_id=1, source_target_pairs={{4,0},{8,4},{12,8},{16,12},{20,16},{24,20},{28,24},{5,1},{9,5},{13... | collective-permute-start | bytes 92168 | tf_op jit(solution)/shard_map/ppermute | solution.py:47
  219.1 31.6 %all-to-all-start.1 = ((bf16[8,256,128]{2,1,0:T(8,128)(2,1)}), bf16[8,256,128]{2,1,0:T(8,128)(2,1)}, u32[]{:S(2)}, u32[]{:S(2)}) async-start(bf16[8,256,128]{2,1,0:T(8,128)(2,1)} %copy-done.25), calls=%async_computation.1 | async-start | bytes 1048576 | tf_op jit(solution)/shard_map/all_to_all | solution.py:122
  (104 other events, 828.2 us)

commit v2 on v1

--- a/solution.py
+++ b/solution.py
@@ -238,13 +238,17 @@
 
 
 def wide_body(at_ref, *refs, groups):
-    pieces, sides, out_ref = refs[: 4 * groups], refs[4 * groups : 5 * groups], refs[5 * groups]
+    pieces, refs = refs[: 4 * groups], refs[4 * groups :]
+    gps, ups = refs[:groups], refs[groups : 2 * groups]
+    gg_ref, ug_ref = refs[2 * groups :]
     share = pieces[0].shape[2]
-    side = join([rows_of(ref) for ref in sides])
+    gp = join([rows_of(ref) for ref in gps])
+    up = join([rows_of(ref) for ref in ups])
     for j in range(4):
         at = pl.ds(pl.multiple_of((at_ref[0] ^ j) * share, share), share)
         rows = join([rows_of(pieces[4 * g + j]) for g in range(groups)])
-        out_ref[at, :] = mm(rows, side, 0, 0)
+        gg_ref[at, :] = mm(rows, gp, 0, 0)
+        ug_ref[at, :] = mm(rows, up, 0, 0)
 
 
 def down_body(at_ref, *refs, groups):
@@ -444,21 +448,18 @@
         args = (*sums[c][0], *sums[c][1])
         totals = call(add, at, args, [((capacity, cols), bf16)] * experts)
         backs.append(sp_exchange(totals))
-    wide = []
-    for sides in (gate_pres, up_pres):
-        wide += call(
-            functools.partial(wide_body, groups=2),
-            at,
-            (*row_groups[0], *row_groups[1], *sides),
-            [((model_width, width), f32)],
-        )
-    gate_grad, up_grad = wide
+    gate_grad, up_grad = call(
+        functools.partial(wide_body, groups=2),
+        at,
+        (*row_groups[0], *row_groups[1], *gate_pres, *up_pres),
+        [((model_width, width), f32)] * 2,
+        keep=False,
+    )
     (down_grad,) = call(
         functools.partial(down_body, groups=2),
         at,
         (*cot_groups[0], *cot_groups[1], *hiddens),
         [((width, model_width), f32)],
-        keep=False,
     )
     for c in range(chunks):
         own = combine(at, picks, cotangent, backs[c], parts[c], share)

time: 254 us -> 226 us (0.89)
  local copies, waits for them, and re-layouts: 22.2 us -> 8.19 us
  waiting for transfers between devices: 82.8 us -> 72.2 us
    unnamed x179 -> x125, local copies, waits for them, and re-layouts: 21.2 us -> 7.9 us
    ppermute x32, waiting for transfers between devices: 45.2 us -> 36.9 us  [tp_swap(): return lax.ppermute(value, 'tp', [(i, i ^ dist) for i in range(count)])]
    ppermute x28, waiting for transfers between devices: 37.5 us -> 31.3 us  [sp_swap(): return lax.ppermute(value, 'sp', [(i, i ^ dist) for i in range(count)])]
    all_to_all x2, waiting for transfers between devices: 0.01 us -> 3.95 us  [sp_all(): return lax.all_to_all(value, 'sp', split_axis=0, concat_axis=0, tiled=True)]
    all_to_all x2, starting transfers between devices: 11.2 us -> 8.59 us  [sp_all(): return lax.all_to_all(value, 'sp', split_axis=0, concat_axis=0, tiled=True)]
    pallas_call x22 -> x21, Pallas kernels: 48.5 us -> 47.7 us  [call(): pl.pallas_call(body, grid_spec=pltpu.PrefetchScalarGridSpec(num_scalar_pr...]
  transfers between devices with their start and end apart: 63 -> 63, of which waited for: 19 -> 23; matrix products, arithmetic and copies ran while one was open for 3% -> 3% of each run, Pallas kernels for 18% -> 20%
where the time goes in v2:
time: 226 us; the launch traced here: 225 us
  starting transfers between devices  87.2 us (39%)
  waiting for transfers between devices  72.2 us (32%)
  Pallas kernels  47.7 us (21%)
  local copies, waits for them, and re-layouts  8.19 us (4%)
  other arithmetic  8.11 us (4%)
    ppermute x28, starting transfers between devices, sp_swap(): return lax.ppermute(value, 'sp', [(i, i ^ dist) for i in range(count)])  57.7 us
    pallas_call x21, Pallas kernels, call(): pl.pallas_call(body, grid_spec=pltpu.PrefetchScalarGridSpec(num_scalar_pr...  47.7 us
    ppermute x32, waiting for transfers between devices, tp_swap(): return lax.ppermute(value, 'tp', [(i, i ^ dist) for i in range(count)])  36.9 us
    ppermute x28, waiting for transfers between devices, sp_swap(): return lax.ppermute(value, 'sp', [(i, i ^ dist) for i in range(count)])  31.3 us
    ppermute x32, starting transfers between devices, tp_swap(): return lax.ppermute(value, 'tp', [(i, i ^ dist) for i in range(count)])  19.6 us
    all_to_all x2, starting transfers between devices, sp_all(): return lax.all_to_all(value, 'sp', split_axis=0, concat_axis=0, tiled=True)  8.59 us
    unnamed x125, local copies, waits for them, and re-layouts  7.9 us
  transfers between devices with their start and end apart: 63, of which 23 were waited for; matrix products, arithmetic and copies ran while one was open for 3% of the time, Pallas kernels for 20%

profile of v2, /device:TPU:0, one launch (start us, length us, event | category | flops | bytes accessed | tf_op | source)
XLA Modules:
  0.0 224.9 jit_solution(10346968210716391329)
XLA Ops:
  1.3 3.4 %shard_map.189 = (bf16[144,512]{1,0:T(8,128)(2,1)}, bf16[144,512]{1,0:T(8,128)(2,1)}, bf16[144,512]{1,0:T(8,128)(2,1)}, bf16[144,512]{1,0:T(8,128)(2,1)}, bf16[1...) custom-call(s32[2]{0:T(128)} %pad_add_fusion.at_ref, ...), custom_call_target="tpu_custom_call" | custom-call | tf_op jit(solution)/shard_map/pallas_call | solution.py:87
  4.7 4.1 %collective-permute-start.2 = (bf16[144,512]{1,0:T(8,128)(2,1)}, bf16[144,512]{1,0:T(8,128)(2,1)S(1)}, u32[]{:S(2)}, u32[]{:S(2)}) collective-permute-start(bf16[144,512]{1,0:T(8,128)(2,1)} %get-tuple-element.71), channel_id=1, source_target_pairs={{0,12},{4,8},{8,4},{12,0},{16,28},{20,24},{24,20},{28,16},{1,13},{... | collective-permute-start | bytes 442376 | tf_op jit(solution)/shard_map/ppermute | solution.py:111
  9.4 4.9 %collective-permute-start.9 = (bf16[144,512]{1,0:T(8,128)(2,1)}, bf16[144,512]{1,0:T(8,128)(2,1)S(1)}, u32[]{:S(2)}, u32[]{:S(2)}) collective-permute-start(bf16[144,512]{1,0:T(8,128)(2,1)} %get-tuple-element.75), channel_id=1, source_target_pairs={{0,28},{4,24},{8,20},{12,16},{16,12},{20,8},{24,4},{28,0},{1,29},{... | collective-permute-start | bytes 442376 | tf_op jit(solution)/shard_map/ppermute | solution.py:111
  14.5 1.6 shard_map.190
  16.1 2.1 collective-permute-start.7
  18.2 1.6 collective-permute-start.6
  19.9 5.9 %collective-permute-start.15 = (bf16[144,512]{1,0:T(8,128)(2,1)S(1)}, bf16[144,512]{1,0:T(8,128)(2,1)S(1)}, u32[]{:S(2)}, u32[]{:S(2)}) collective-permute-start(bf16[144,512]{1,0:T(8,128)(2,1)S(1)} %get-tuple-element.79), channel_id=1, source_target_pairs={{0,12},{4,8},{8,4},{12,0},{16,28},{20,24},{24,20},{28,16},{1,13},{... | collective-permute-start | bytes 442376 | tf_op jit(solution)/shard_map/ppermute | solution.py:111
  26.0 1.6 collective-permute-start.4
  27.5 9.8 %collective-permute-done.7 = bf16[144,512]{1,0:T(8,128)(2,1)S(1)} collective-permute-done((bf16[144,512]{1,0:T(8,128)(2,1)S(1)}, bf16[144,512]{1,0:T(8,128)(2,1)S(1)}, u32[]{:S(2)}, u32[]{:S(2)}) %collective-permute-start.7) | collective-permute-done | bytes 147488 | tf_op jit(solution)/shard_map/ppermute | solution.py:111
  37.4 1.7 collective-permute-done.6
  39.6 3.4 %collective-permute-start.22 = (bf16[144,512]{1,0:T(8,128)(2,1)S(1)}, bf16[144,512]{1,0:T(8,128)(2,1)S(1)}, u32[]{:S(2)}, u32[]{:S(2)}) collective-permute-start(bf16[144,512]{1,0:T(8,128)(2,1)S(1)} %get-tuple-element.86), channel_id=1, source_target_pairs={{0,28},{4,24},{8,20},{12,16},{16,12},{20,8},{24,4},{28,0},{1,29},{... | collective-permute-start | bytes 442376 | tf_op jit(solution)/shard_map/ppermute | solution.py:111
  43.0 1.9 collective-permute-start.21
  45.8 2.2 collective-permute-start.20
  49.1 9.8 %collective-permute-start.19 = (bf16[144,512]{1,0:T(8,128)(2,1)S(1)}, bf16[144,512]{1,0:T(8,128)(2,1)S(1)}, u32[]{:S(2)}, u32[]{:S(2)}) collective-permute-start(bf16[144,512]{1,0:T(8,128)(2,1)S(1)} %get-tuple-element.83), channel_id=1, source_target_pairs={{0,16},{4,20},{8,24},{12,28},{16,0},{20,4},{24,8},{28,12},{1,17},{... | collective-permute-start | bytes 442376 | tf_op jit(solution)/shard_map/ppermute | solution.py:111
  59.0 1.6 collective-permute-start.17
  60.7 3.8 %collective-permute-done.20 = bf16[144,512]{1,0:T(8,128)(2,1)S(1)} collective-permute-done((bf16[144,512]{1,0:T(8,128)(2,1)S(1)}, bf16[144,512]{1,0:T(8,128)(2,1)S(1)}, u32[]{:S(2)}, u32[]{:S(2)}) %collective-permute-start.20) | collective-permute-done | bytes 147488 | tf_op jit(solution)/shard_map/ppermute | solution.py:111
  68.2 2.2 collective-permute-done.17.p2.refs_2_
  70.4 12.6 %collective-permute-done.11.p2.refs_6_ = bf16[4,144,512]{2,1,0:T(8,128)(2,1)S(1)} collective-permute-done((bf16[4,144,512]{2,1,0:T(8,128)(2,1)S(1)}, bf16[4,144,512]{2,1,0:T(8,128)(2,1)S(1)}, u32[]{:S(2)}, u32[]{:S(2)}) %collective-permute-start.11) | collective-permute-done | bytes 589856 | tf_op jit(solution)/shard_map/ppermute | solution.py:36
  83.6 10.7 %collective-permute-done.24.p2.refs_6_ = bf16[4,144,512]{2,1,0:T(8,128)(2,1)S(1)} collective-permute-done((bf16[4,144,512]{2,1,0:T(8,128)(2,1)S(1)}, bf16[4,144,512]{2,1,0:T(8,128)(2,1)S(1)}, u32[]{:S(2)}, u32[]{:S(2)}) %collective-permute-start.24) | collective-permute-done | bytes 589856 | tf_op jit(solution)/shard_map/ppermute | solution.py:36
  94.8 2.3 %shard_map.191 = (f32[4,144,256]{2,1,0:T(8,128)S(1)}, f32[4,144,256]{2,1,0:T(8,128)S(1)}) custom-call(s32[2]{0:T(128)S(1)} %copy-done.42, bf16[4,144,512]{2,1,0:T(8,128)(2,1)S(1)} %pad_maximum_fusion.p0.refs_0_, bf16[4,144,512]{2,1,0:T(8,128)(2,1)S(1)} %collective-permute-done.3.p1.refs_1_, bf16[4,144,512]{2,1,0:T(8,128)(2,1)S(1)} %collective-permute-done.4.p2.refs_2_, ...), custom_call_target="tpu_custom_call" | custom-call | tf_op jit(solution)/shard_map/pallas_call | solution.py:87
  97.2 1.7 shard_map.192
  99.6 2.0 shard_map.198
  101.8 2.1 shard_map.193
  104.0 1.7 shard_map.194
  106.6 2.0 shard_map.199
  109.7 1.6 collective-permute-start.41
  116.8 2.8 %collective-permute-done.41.refs_2_ = bf16[4,144,256]{2,1,0:T(8,128)(2,1)S(1)} collective-permute-done((bf16[4,144,256]{2,1,0:T(8,128)(2,1)S(1)}, bf16[4,144,256]{2,1,0:T(8,128)(2,1)S(1)}, u32[]{:S(2)}, u32[]{:S(2)}) %collective-permute-start.41) | collective-permute-done | bytes 294944 | tf_op jit(solution)/shard_map/ppermute | solution.py:36
  119.6 6.3 %collective-permute-done.43.refs_5_ = bf16[4,144,256]{2,1,0:T(8,128)(2,1)S(1)} collective-permute-done((bf16[4,144,256]{2,1,0:T(8,128)(2,1)S(1)}, bf16[4,144,256]{2,1,0:T(8,128)(2,1)S(1)}, u32[]{:S(2)}, u32[]{:S(2)}) %collective-permute-start.43) | collective-permute-done | bytes 294944 | tf_op jit(solution)/shard_map/ppermute | solution.py:36
  128.6 1.7 collective-permute-start.45
  131.6 3.8 %collective-permute-start.47 = (bf16[144,256]{1,0:T(8,128)(2,1)S(1)}, bf16[144,256]{1,0:T(8,128)(2,1)S(1)}, u32[]{:S(2)}, u32[]{:S(2)}) collective-permute-start(bf16[144,256]{1,0:T(8,128)(2,1)S(1)} %get-tuple-element.120), channel_id=1, source_target_pairs={{0,16},{4,20},{8,24},{12,28},{16,0},{20,4},{24,8},{28,12},{1,17},{... | collective-permute-start | bytes 221192 | tf_op jit(solution)/shard_map/ppermute | solution.py:111
  135.4 1.6 collective-permute-start.48
  137.0 1.6 collective-permute-start.49
  138.6 2.6 %collective-permute-done.47.refs_4_ = bf16[144,256]{1,0:T(8,128)(2,1)S(1)} collective-permute-done((bf16[144,256]{1,0:T(8,128)(2,1)S(1)}, bf16[144,256]{1,0:T(8,128)(2,1)S(1)}, u32[]{:S(2)}, u32[]{:S(2)}) %collective-permute-start.47) | collective-permute-done | bytes 73760 | tf_op jit(solution)/shard_map/ppermute | solution.py:111
  145.6 3.4 %collective-permute-done.50.refs_7_ = bf16[144,256]{1,0:T(8,128)(2,1)S(1)} collective-permute-done((bf16[144,256]{1,0:T(8,128)(2,1)}, bf16[144,256]{1,0:T(8,128)(2,1)S(1)}, u32[]{:S(2)}, u32[]{:S(2)}) %collective-permute-start.50) | collective-permute-done | bytes 73760 | tf_op jit(solution)/shard_map/ppermute | solution.py:111
  155.0 1.8 shard_map.200
  158.3 2.1 collective-permute-start.32
  160.4 1.6 collective-permute-done.30.refs_1_
  162.0 2.1 collective-permute-start.34
  164.4 3.7 %collective-permute-start.36 = (bf16[144,256]{1,0:T(8,128)(2,1)S(1)}, bf16[144,256]{1,0:T(8,128)(2,1)S(1)}, u32[]{:S(2)}, u32[]{:S(2)}) collective-permute-start(bf16[144,256]{1,0:T(8,128)(2,1)S(1)} %get-tuple-element.109), channel_id=1, source_target_pairs={{0,28},{4,24},{8,20},{12,16},{16,12},{20,8},{24,4},{28,0},{1,29},{... | collective-permute-start | bytes 221192 | tf_op jit(solution)/shard_map/ppermute | solution.py:111
  181.0 2.0 shard_map.208
  183.1 5.0 %all-to-all-start.1 = ((bf16[8,256,128]{2,1,0:T(8,128)(2,1)}), bf16[8,256,128]{2,1,0:T(8,128)(2,1)}, u32[]{:S(2)}, u32[]{:S(2)}) async-start(bf16[8,256,128]{2,1,0:T(8,128)(2,1)} %shard_map.208), calls=%async_computation.1 | async-start | bytes 1048576 | tf_op jit(solution)/shard_map/all_to_all | solution.py:122
  188.1 4.2 %shard_map.206 = (bf16[384,2048]{1,0:T(8,128)(2,1)}, f32[384,256]{1,0:T(8,128)S(1)}, f32[2,384]{1,0:T(2,128)S(1)}) custom-call(s32[2]{0:T(128)S(1)} %copy-done.42, bf16[384,256]{1,0:T(8,128)(2,1)S(1)} %shard_map.201.refs_0_.p0, bf16[384,256]{1,0:T(8,128)(2,1)S(1)} %collective-permute-done.37.refs_1_.p1, ...), custom_call_target="tpu_custom_call" | custom-call | tf_op jit(solution)/shard_map/pallas_call | solution.py:87
  194.4 3.0 %shard_map.207 = bf16[8,256,128]{2,1,0:T(8,128)(2,1)} custom-call(s32[2]{0:T(128)S(1)} %copy-done.42, bf16[384,256]{1,0:T(8,128)(2,1)S(1)} %shard_map.201.refs_0_.p0, bf16[384,256]{1,0:T(8,128)(2,1)S(1)} %collective-permute-done.37.refs_1_.p1, bf16[384,256]{1,0:T(8,128)(2,1)S(1)} %collective-permute-done.38.refs_2_.p2, ...), custom_call_target="tpu_custom_call" | custom-call | tf_op jit(solution)/shard_map/pallas_call | solution.py:87
  199.1 3.9 %all-to-all-done.1 = bf16[8,256,128]{2,1,0:T(8,128)(2,1)} async-done(((bf16[8,256,128]{2,1,0:T(8,128)(2,1)}), bf16[8,256,128]{2,1,0:T(8,128)(2,1)}, u32[]{:S(2)}, u32[]{:S(2)}) %all-to-all-start.1) | async-done | bytes 524320 | tf_op jit(solution)/shard_map/all_to_all | solution.py:122
  203.0 3.6 %all-to-all-start = ((bf16[8,256,128]{2,1,0:T(8,128)(2,1)}), bf16[8,256,128]{2,1,0:T(8,128)(2,1)S(1)}, u32[]{:S(2)}, u32[]{:S(2)}) async-start(bf16[8,256,128]{2,1,0:T(8,128)(2,1)} %shard_map.207), calls=%async_computation | async-start | bytes 1048576 | tf_op jit(solution)/shard_map/all_to_all | solution.py:122
  207.4 8.8 %shard_map.195 = (f32[2048,256]{1,0:T(8,128)}, f32[2048,256]{1,0:T(8,128)}) custom-call(s32[2]{0:T(128)} %pad_add_fusion.at_ref, bf16[4,144,512]{2,1,0:T(8,128)(2,1)} %copy-done.3, bf16[4,144,512]{2,1,0:T(8,128)(2,1)} %copy-done.9, bf16[4,144,512]{2,1,0:T(8,128)(2,1)} %copy-done.10, bf16[4,144,512]{2,1,0:T(8,128)(2,1)} %copy-done.12, ...), custom_call_target="tpu_custom_call" | custom-call | tf_op jit(solution)/shard_map/pallas_call | solution.py:87
  216.3 3.4 %shard_map.196 = f32[256,2048]{1,0:T(8,128)} custom-call(s32[2]{0:T(128)S(1)} %copy-done.43, bf16[4,144,512]{2,1,0:T(8,128)(2,1)S(1)} %pad_maximum_fusion.2.p0.refs_0_, bf16[4,144,512]{2,1,0:T(8,128)(2,1)S(1)} %copy-done.18, bf16[4,144,512]{2,1,0:T(8,128)(2,1)S(1)} %copy-done.16, bf16[4,144,512]{2,1,0:T(8,128)(2,1)S(1)} %copy-done.22, ...), custom_call_target="tpu_custom_call" | custom-call | tf_op jit(solution)/shard_map/pallas_call | solution.py:87
  219.7 2.5 %multiply_convert_fusion = (bf16[384,256]{1,0:T(8,128)(2,1)}, f32[384,256]{1,0:T(8,128)S(1)}) fusion(f32[384,256]{1,0:T(8,128)S(1)} %get-tuple-element.128, f32[384,256]{1,0:T(8,128)S(1)} %subtract_multiply_fusion, f32[256]{0:T(256)S(1)} %bitcast.125, f32[30,256]{1,0:T(8,128)S(1)} %collective-permute-done.60, f32[256]{0:T(256)S(1)} %bitcast.126, ...), kind=kLoop, calls=%fused_computation.154 | loop fusion | flops 9142272 | bytes 1438720 | tf_op jit(solution)/shard_map/convert_element_type | solution.py:498
  (245 shorter events, 53.5 us)
Async XLA Ops:
  4.7 11.4 %collective-permute-start.2 = (bf16[144,512]{1,0:T(8,128)(2,1)}, bf16[144,512]{1,0:T(8,128)(2,1)S(1)}, u32[]{:S(2)}, u32[]{:S(2)}) collective-permute-start(bf16[144,512]{1,0:T(8,128)(2,1)} %get-tuple-element.71), channel_id=1, source_target_pairs={{0,12},{4,8},{8,4},{12,0},{16,28},{20,24},{24,20},{28,16},{1,13},{... | collective-permute-start | bytes 442376 | tf_op jit(solution)/shard_map/ppermute | solution.py:111
  8.8 9.5 %collective-permute-start.1 = (bf16[144,512]{1,0:T(8,128)(2,1)}, bf16[144,512]{1,0:T(8,128)(2,1)S(1)}, u32[]{:S(2)}, u32[]{:S(2)}) collective-permute-start(bf16[144,512]{1,0:T(8,128)(2,1)} %get-tuple-element.70), channel_id=1, source_target_pairs={{0,8},{4,12},{8,0},{12,4},{16,24},{20,28},{24,16},{28,20},{1,9},{5... | collective-permute-start | bytes 442376 | tf_op jit(solution)/shard_map/ppermute | solution.py:111
  9.2 10.7 %collective-permute-start = (bf16[144,512]{1,0:T(8,128)(2,1)}, bf16[144,512]{1,0:T(8,128)(2,1)S(1)}, u32[]{:S(2)}, u32[]{:S(2)}) collective-permute-start(bf16[144,512]{1,0:T(8,128)(2,1)} %get-tuple-element.69), channel_id=1, source_target_pairs={{0,4},{4,0},{8,12},{12,8},{16,20},{20,16},{24,28},{28,24},{1,5},{5... | collective-permute-start | bytes 442376 | tf_op jit(solution)/shard_map/ppermute | solution.py:111
  9.4 16.5 %collective-permute-start.9 = (bf16[144,512]{1,0:T(8,128)(2,1)}, bf16[144,512]{1,0:T(8,128)(2,1)S(1)}, u32[]{:S(2)}, u32[]{:S(2)}) collective-permute-start(bf16[144,512]{1,0:T(8,128)(2,1)} %get-tuple-element.75), channel_id=1, source_target_pairs={{0,28},{4,24},{8,20},{12,16},{16,12},{20,8},{24,4},{28,0},{1,29},{... | collective-permute-start | bytes 442376 | tf_op jit(solution)/shard_map/ppermute | solution.py:111
  14.3 11.7 %collective-permute-start.8 = (bf16[144,512]{1,0:T(8,128)(2,1)}, bf16[144,512]{1,0:T(8,128)(2,1)S(1)}, u32[]{:S(2)}, u32[]{:S(2)}) collective-permute-start(bf16[144,512]{1,0:T(8,128)(2,1)} %get-tuple-element.74), channel_id=1, source_target_pairs={{0,24},{4,28},{8,16},{12,20},{16,8},{20,12},{24,0},{28,4},{1,25},{... | collective-permute-start | bytes 442376 | tf_op jit(solution)/shard_map/ppermute | solution.py:111
  16.1 21.2 %collective-permute-start.7 = (bf16[144,512]{1,0:T(8,128)(2,1)S(1)}, bf16[144,512]{1,0:T(8,128)(2,1)S(1)}, u32[]{:S(2)}, u32[]{:S(2)}) collective-permute-start(bf16[144,512]{1,0:T(8,128)(2,1)S(1)} %copy-done.61), channel_id=1, source_target_pairs={{0,20},{4,16},{8,28},{12,24},{16,4},{20,0},{24,12},{28,8},{1,21},{... | collective-permute-start | bytes 442376 | tf_op jit(solution)/shard_map/ppermute | solution.py:111
  18.2 20.9 %collective-permute-start.6 = (bf16[144,512]{1,0:T(8,128)(2,1)S(1)}, bf16[144,512]{1,0:T(8,128)(2,1)S(1)}, u32[]{:S(2)}, u32[]{:S(2)}) collective-permute-start(bf16[144,512]{1,0:T(8,128)(2,1)S(1)} %copy-done.60), channel_id=1, source_target_pairs={{0,16},{4,20},{8,24},{12,28},{16,0},{20,4},{24,8},{28,12},{1,17},{... | collective-permute-start | bytes 442376 | tf_op jit(solution)/shard_map/ppermute | solution.py:111
  19.9 19.8 %collective-permute-start.15 = (bf16[144,512]{1,0:T(8,128)(2,1)S(1)}, bf16[144,512]{1,0:T(8,128)(2,1)S(1)}, u32[]{:S(2)}, u32[]{:S(2)}) collective-permute-start(bf16[144,512]{1,0:T(8,128)(2,1)S(1)} %get-tuple-element.79), channel_id=1, source_target_pairs={{0,12},{4,8},{8,4},{12,0},{16,28},{20,24},{24,20},{28,16},{1,13},{... | collective-permute-start | bytes 442376 | tf_op jit(solution)/shard_map/ppermute | solution.py:111
  25.9 41.7 %collective-permute-start.3 = (bf16[4,144,512]{2,1,0:T(8,128)(2,1)S(1)}, bf16[4,144,512]{2,1,0:T(8,128)(2,1)S(1)}, u32[]{:S(2)}, u32[]{:S(2)}) collective-permute-start(bf16[4,144,512]{2,1,0:T(8,128)(2,1)S(1)} %pad_maximum_fusion.p0.refs_0_), channel_id=1, source_target_pairs={{0,1},{1,0},{2,3},{3,2},{4,5},{5,4},{6,7},{7,6},{8,9},{9,8},{10,11... | collective-permute-start | bytes 1769480 | tf_op jit(solution)/shard_map/ppermute | solution.py:36
  26.0 42.2 %collective-permute-start.4 = (bf16[4,144,512]{2,1,0:T(8,128)(2,1)S(1)}, bf16[4,144,512]{2,1,0:T(8,128)(2,1)S(1)}, u32[]{:S(2)}, u32[]{:S(2)}) collective-permute-start(bf16[4,144,512]{2,1,0:T(8,128)(2,1)S(1)} %pad_maximum_fusion.p0.refs_0_), channel_id=1, source_target_pairs={{0,2},{1,3},{2,0},{3,1},{4,6},{5,7},{6,4},{7,5},{8,10},{9,11},{10,... | collective-permute-start | bytes 1769480 | tf_op jit(solution)/shard_map/ppermute | solution.py:36
  39.1 6.7 %collective-permute-start.13 = (bf16[144,512]{1,0:T(8,128)(2,1)S(1)}, bf16[144,512]{1,0:T(8,128)(2,1)S(1)}, u32[]{:S(2)}, u32[]{:S(2)}) collective-permute-start(bf16[144,512]{1,0:T(8,128)(2,1)S(1)} %get-tuple-element.77), channel_id=1, source_target_pairs={{0,4},{4,0},{8,12},{12,8},{16,20},{20,16},{24,28},{28,24},{1,5},{5... | collective-permute-start | bytes 442376 | tf_op jit(solution)/shard_map/ppermute | solution.py:111
  39.6 9.5 %collective-permute-start.22 = (bf16[144,512]{1,0:T(8,128)(2,1)S(1)}, bf16[144,512]{1,0:T(8,128)(2,1)S(1)}, u32[]{:S(2)}, u32[]{:S(2)}) collective-permute-start(bf16[144,512]{1,0:T(8,128)(2,1)S(1)} %get-tuple-element.86), channel_id=1, source_target_pairs={{0,28},{4,24},{8,20},{12,16},{16,12},{20,8},{24,4},{28,0},{1,29},{... | collective-permute-start | bytes 442376 | tf_op jit(solution)/shard_map/ppermute | solution.py:111
  43.0 16.0 %collective-permute-start.21 = (bf16[144,512]{1,0:T(8,128)(2,1)S(1)}, bf16[144,512]{1,0:T(8,128)(2,1)S(1)}, u32[]{:S(2)}, u32[]{:S(2)}) collective-permute-start(bf16[144,512]{1,0:T(8,128)(2,1)S(1)} %get-tuple-element.85), channel_id=1, source_target_pairs={{0,24},{4,28},{8,16},{12,20},{16,8},{20,12},{24,0},{28,4},{1,25},{... | collective-permute-start | bytes 442376 | tf_op jit(solution)/shard_map/ppermute | solution.py:111
  45.8 18.6 %collective-permute-start.20 = (bf16[144,512]{1,0:T(8,128)(2,1)S(1)}, bf16[144,512]{1,0:T(8,128)(2,1)S(1)}, u32[]{:S(2)}, u32[]{:S(2)}) collective-permute-start(bf16[144,512]{1,0:T(8,128)(2,1)S(1)} %get-tuple-element.84), channel_id=1, source_target_pairs={{0,20},{4,16},{8,28},{12,24},{16,4},{20,0},{24,12},{28,8},{1,21},{... | collective-permute-start | bytes 442376 | tf_op jit(solution)/shard_map/ppermute | solution.py:111
  49.1 16.9 %collective-permute-start.19 = (bf16[144,512]{1,0:T(8,128)(2,1)S(1)}, bf16[144,512]{1,0:T(8,128)(2,1)S(1)}, u32[]{:S(2)}, u32[]{:S(2)}) collective-permute-start(bf16[144,512]{1,0:T(8,128)(2,1)S(1)} %get-tuple-element.83), channel_id=1, source_target_pairs={{0,16},{4,20},{8,24},{12,28},{16,0},{20,4},{24,8},{28,12},{1,17},{... | collective-permute-start | bytes 442376 | tf_op jit(solution)/shard_map/ppermute | solution.py:111
  59.0 11.4 %collective-permute-start.17 = (bf16[4,144,512]{2,1,0:T(8,128)(2,1)S(1)}, bf16[4,144,512]{2,1,0:T(8,128)(2,1)S(1)}, u32[]{:S(2)}, u32[]{:S(2)}) collective-permute-start(bf16[4,144,512]{2,1,0:T(8,128)(2,1)S(1)} %pad_maximum_fusion.2.p0.refs_0_), channel_id=1, source_target_pairs={{0,2},{1,3},{2,0},{3,1},{4,6},{5,7},{6,4},{7,5},{8,10},{9,11},{10,... | collective-permute-start | bytes 1769480 | tf_op jit(solution)/shard_map/ppermute | solution.py:36
  64.5 18.6 %collective-permute-start.16 = (bf16[4,144,512]{2,1,0:T(8,128)(2,1)S(1)}, bf16[4,144,512]{2,1,0:T(8,128)(2,1)S(1)}, u32[]{:S(2)}, u32[]{:S(2)}) collective-permute-start(bf16[4,144,512]{2,1,0:T(8,128)(2,1)S(1)} %pad_maximum_fusion.2.p0.refs_0_), channel_id=1, source_target_pairs={{0,1},{1,0},{2,3},{3,2},{4,5},{5,4},{6,7},{7,6},{8,9},{9,8},{10,11... | collective-permute-start | bytes 1769480 | tf_op jit(solution)/shard_map/ppermute | solution.py:36
  66.0 17.1 %collective-permute-start.11 = (bf16[4,144,512]{2,1,0:T(8,128)(2,1)S(1)}, bf16[4,144,512]{2,1,0:T(8,128)(2,1)S(1)}, u32[]{:S(2)}, u32[]{:S(2)}) collective-permute-start(bf16[4,144,512]{2,1,0:T(8,128)(2,1)S(1)} %pad_maximum_fusion.1.p0.refs_4_), channel_id=1, source_target_pairs={{0,2},{1,3},{2,0},{3,1},{4,6},{5,7},{6,4},{7,5},{8,10},{9,11},{10,... | collective-permute-start | bytes 1769480 | tf_op jit(solution)/shard_map/ppermute | solution.py:36
  67.6 26.7 %collective-permute-start.24 = (bf16[4,144,512]{2,1,0:T(8,128)(2,1)S(1)}, bf16[4,144,512]{2,1,0:T(8,128)(2,1)S(1)}, u32[]{:S(2)}, u32[]{:S(2)}) collective-permute-start(bf16[4,144,512]{2,1,0:T(8,128)(2,1)S(1)} %pad_maximum_fusion.3.p0.refs_4_), channel_id=1, source_target_pairs={{0,2},{1,3},{2,0},{3,1},{4,6},{5,7},{6,4},{7,5},{8,10},{9,11},{10,... | collective-permute-start | bytes 1769480 | tf_op jit(solution)/shard_map/ppermute | solution.py:36
  68.2 26.1 %collective-permute-start.5 = (bf16[4,144,512]{2,1,0:T(8,128)(2,1)S(1)}, bf16[4,144,512]{2,1,0:T(8,128)(2,1)S(1)}, u32[]{:S(2)}, u32[]{:S(2)}) collective-permute-start(bf16[4,144,512]{2,1,0:T(8,128)(2,1)S(1)} %collective-permute-done.4.p2.refs_2_), channel_id=1, source_target_pairs={{0,1},{1,0},{2,3},{3,2},{4,5},{5,4},{6,7},{7,6},{8,9},{9,8},{10,11... | collective-permute-start | bytes 1769480 | tf_op jit(solution)/shard_map/ppermute | solution.py:36
  70.4 26.7 %collective-permute-start.18 = (bf16[4,144,512]{2,1,0:T(8,128)(2,1)S(1)}, bf16[4,144,512]{2,1,0:T(8,128)(2,1)S(1)}, u32[]{:S(2)}, u32[]{:S(2)}) collective-permute-start(bf16[4,144,512]{2,1,0:T(8,128)(2,1)S(1)} %collective-permute-done.17.p2.refs_2_), channel_id=1, source_target_pairs={{0,1},{1,0},{2,3},{3,2},{4,5},{5,4},{6,7},{7,6},{8,9},{9,8},{10,11... | collective-permute-start | bytes 1769480 | tf_op jit(solution)/shard_map/ppermute | solution.py:36
  83.1 18.6 %collective-permute-start.10 = (bf16[4,144,512]{2,1,0:T(8,128)(2,1)S(1)}, bf16[4,144,512]{2,1,0:T(8,128)(2,1)S(1)}, u32[]{:S(2)}, u32[]{:S(2)}) collective-permute-start(bf16[4,144,512]{2,1,0:T(8,128)(2,1)S(1)} %pad_maximum_fusion.1.p0.refs_4_), channel_id=1, source_target_pairs={{0,1},{1,0},{2,3},{3,2},{4,5},{5,4},{6,7},{7,6},{8,9},{9,8},{10,11... | collective-permute-start | bytes 1769480 | tf_op jit(solution)/shard_map/ppermute | solution.py:36
  83.1 18.6 %collective-permute-start.12 = (bf16[4,144,512]{2,1,0:T(8,128)(2,1)S(1)}, bf16[4,144,512]{2,1,0:T(8,128)(2,1)S(1)}, u32[]{:S(2)}, u32[]{:S(2)}) collective-permute-start(bf16[4,144,512]{2,1,0:T(8,128)(2,1)S(1)} %collective-permute-done.11.p2.refs_6_), channel_id=1, source_target_pairs={{0,1},{1,0},{2,3},{3,2},{4,5},{5,4},{6,7},{7,6},{8,9},{9,8},{10,11... | collective-permute-start | bytes 1769480 | tf_op jit(solution)/shard_map/ppermute | solution.py:36
  94.3 9.7 %collective-permute-start.23 = (bf16[4,144,512]{2,1,0:T(8,128)(2,1)S(1)}, bf16[4,144,512]{2,1,0:T(8,128)(2,1)S(1)}, u32[]{:S(2)}, u32[]{:S(2)}) collective-permute-start(bf16[4,144,512]{2,1,0:T(8,128)(2,1)S(1)} %pad_maximum_fusion.3.p0.refs_4_), channel_id=1, source_target_pairs={{0,1},{1,0},{2,3},{3,2},{4,5},{5,4},{6,7},{7,6},{8,9},{9,8},{10,11... | collective-permute-start | bytes 1769480 | tf_op jit(solution)/shard_map/ppermute | solution.py:36
  94.3 9.7 %collective-permute-start.25 = (bf16[4,144,512]{2,1,0:T(8,128)(2,1)S(1)}, bf16[4,144,512]{2,1,0:T(8,128)(2,1)S(1)}, u32[]{:S(2)}, u32[]{:S(2)}) collective-permute-start(bf16[4,144,512]{2,1,0:T(8,128)(2,1)S(1)} %collective-permute-done.24.p2.refs_6_), channel_id=1, source_target_pairs={{0,1},{1,0},{2,3},{3,2},{4,5},{5,4},{6,7},{7,6},{8,9},{9,8},{10,11... | collective-permute-start | bytes 1769480 | tf_op jit(solution)/shard_map/ppermute | solution.py:36
  101.6 8.0 %collective-permute-start.40 = (bf16[8,144,256]{2,1,0:T(8,128)(2,1)S(1)}, bf16[8,144,256]{2,1,0:T(8,128)(2,1)S(1)}, u32[]{:S(2)}, u32[]{:S(2)}) collective-permute-start(bf16[8,144,256]{2,1,0:T(8,128)(2,1)S(1)} %get-tuple-element.111), channel_id=1, source_target_pairs={{0,1},{1,0},{2,3},{3,2},{4,5},{5,4},{6,7},{7,6},{8,9},{9,8},{10,11... | collective-permute-start | bytes 1769480 | tf_op jit(solution)/shard_map/ppermute | solution.py:36
  109.7 9.9 %collective-permute-start.41 = (bf16[4,144,256]{2,1,0:T(8,128)(2,1)S(1)}, bf16[4,144,256]{2,1,0:T(8,128)(2,1)S(1)}, u32[]{:S(2)}, u32[]{:S(2)}) collective-permute-start(bf16[4,144,256]{2,1,0:T(8,128)(2,1)S(1)} %add_convert_fusion.1), channel_id=1, source_target_pairs={{0,2},{1,3},{2,0},{3,1},{4,6},{5,7},{6,4},{7,5},{8,10},{9,11},{10,... | collective-permute-start | bytes 884744 | tf_op jit(solution)/shard_map/ppermute | solution.py:36
  111.3 14.6 %collective-permute-start.43 = (bf16[4,144,256]{2,1,0:T(8,128)(2,1)S(1)}, bf16[4,144,256]{2,1,0:T(8,128)(2,1)S(1)}, u32[]{:S(2)}, u32[]{:S(2)}) collective-permute-start(bf16[4,144,256]{2,1,0:T(8,128)(2,1)S(1)} %add_convert_fusion), channel_id=1, source_target_pairs={{0,2},{1,3},{2,0},{3,1},{4,6},{5,7},{6,4},{7,5},{8,10},{9,11},{10,... | collective-permute-start | bytes 884744 | tf_op jit(solution)/shard_map/ppermute | solution.py:36
  113.1 41.9 %collective-permute-start.27 = (bf16[4,144,256]{2,1,0:T(8,128)(2,1)}, bf16[4,144,256]{2,1,0:T(8,128)(2,1)}, u32[]{:S(2)}, u32[]{:S(2)}) collective-permute-start(bf16[4,144,256]{2,1,0:T(8,128)(2,1)} %add_convert_fusion.3), channel_id=1, source_target_pairs={{0,2},{1,3},{2,0},{3,1},{4,6},{5,7},{6,4},{7,5},{8,10},{9,11},{10,... | collective-permute-start | bytes 884744 | tf_op jit(solution)/shard_map/ppermute | solution.py:36
  115.8 39.2 %collective-permute-start.29 = (bf16[4,144,256]{2,1,0:T(8,128)(2,1)}, bf16[4,144,256]{2,1,0:T(8,128)(2,1)}, u32[]{:S(2)}, u32[]{:S(2)}) collective-permute-start(bf16[4,144,256]{2,1,0:T(8,128)(2,1)} %add_convert_fusion.2), channel_id=1, source_target_pairs={{0,2},{1,3},{2,0},{3,1},{4,6},{5,7},{6,4},{7,5},{8,10},{9,11},{10,... | collective-permute-start | bytes 884744 | tf_op jit(solution)/shard_map/ppermute | solution.py:36
  128.6 6.8 %collective-permute-start.45 = (bf16[144,256]{1,0:T(8,128)(2,1)S(1)}, bf16[144,256]{1,0:T(8,128)(2,1)S(1)}, u32[]{:S(2)}, u32[]{:S(2)}) collective-permute-start(bf16[144,256]{1,0:T(8,128)(2,1)S(1)} %get-tuple-element.118), channel_id=1, source_target_pairs={{0,8},{4,12},{8,0},{12,4},{16,24},{20,28},{24,16},{28,20},{1,9},{5... | collective-permute-start | bytes 221192 | tf_op jit(solution)/shard_map/ppermute | solution.py:111
  130.4 6.6 %collective-permute-start.46 = (bf16[144,256]{1,0:T(8,128)(2,1)S(1)}, bf16[144,256]{1,0:T(8,128)(2,1)S(1)}, u32[]{:S(2)}, u32[]{:S(2)}) collective-permute-start(bf16[144,256]{1,0:T(8,128)(2,1)S(1)} %get-tuple-element.119), channel_id=1, source_target_pairs={{0,12},{4,8},{8,4},{12,0},{16,28},{20,24},{24,20},{28,16},{1,13},{... | collective-permute-start | bytes 221192 | tf_op jit(solution)/shard_map/ppermute | solution.py:111
  131.6 9.6 %collective-permute-start.47 = (bf16[144,256]{1,0:T(8,128)(2,1)S(1)}, bf16[144,256]{1,0:T(8,128)(2,1)S(1)}, u32[]{:S(2)}, u32[]{:S(2)}) collective-permute-start(bf16[144,256]{1,0:T(8,128)(2,1)S(1)} %get-tuple-element.120), channel_id=1, source_target_pairs={{0,16},{4,20},{8,24},{12,28},{16,0},{20,4},{24,8},{28,12},{1,17},{... | collective-permute-start | bytes 221192 | tf_op jit(solution)/shard_map/ppermute | solution.py:111
  135.4 9.0 %collective-permute-start.48 = (bf16[144,256]{1,0:T(8,128)(2,1)}, bf16[144,256]{1,0:T(8,128)(2,1)S(1)}, u32[]{:S(2)}, u32[]{:S(2)}) collective-permute-start(bf16[144,256]{1,0:T(8,128)(2,1)} %get-tuple-element.121), channel_id=1, source_target_pairs={{0,20},{4,16},{8,28},{12,24},{16,4},{20,0},{24,12},{28,8},{1,21},{... | collective-permute-start | bytes 221192 | tf_op jit(solution)/shard_map/ppermute | solution.py:111
  137.0 8.0 %collective-permute-start.49 = (bf16[144,256]{1,0:T(8,128)(2,1)}, bf16[144,256]{1,0:T(8,128)(2,1)S(1)}, u32[]{:S(2)}, u32[]{:S(2)}) collective-permute-start(bf16[144,256]{1,0:T(8,128)(2,1)} %get-tuple-element.122), channel_id=1, source_target_pairs={{0,24},{4,28},{8,16},{12,20},{16,8},{20,12},{24,0},{28,4},{1,25},{... | collective-permute-start | bytes 221192 | tf_op jit(solution)/shard_map/ppermute | solution.py:111
  141.8 7.3 %collective-permute-start.50 = (bf16[144,256]{1,0:T(8,128)(2,1)}, bf16[144,256]{1,0:T(8,128)(2,1)S(1)}, u32[]{:S(2)}, u32[]{:S(2)}) collective-permute-start(bf16[144,256]{1,0:T(8,128)(2,1)} %get-tuple-element.123), channel_id=1, source_target_pairs={{0,28},{4,24},{8,20},{12,16},{16,12},{20,8},{24,4},{28,0},{1,29},{... | collective-permute-start | bytes 221192 | tf_op jit(solution)/shard_map/ppermute | solution.py:111
  153.5 19.7 %collective-permute-start.52 = (bf16[384,256]{1,0:T(8,128)(2,1)S(1)}, bf16[384,256]{1,0:T(8,128)(2,1)S(1)}, u32[]{:S(2)}, u32[]{:S(2)}) collective-permute-start(bf16[384,256]{1,0:T(8,128)(2,1)S(1)} %shard_map.203.refs_4_.p0), channel_id=1, source_target_pairs={{0,2},{1,3},{2,0},{3,1},{4,6},{5,7},{6,4},{7,5},{8,10},{9,11},{10,... | collective-permute-start | bytes 589832 | tf_op jit(solution)/shard_map/ppermute | solution.py:36
  160.4 7.7 %collective-permute-start.33 = (bf16[144,256]{1,0:T(8,128)(2,1)S(1)}, bf16[144,256]{1,0:T(8,128)(2,1)S(1)}, u32[]{:S(2)}, u32[]{:S(2)}) collective-permute-start(bf16[144,256]{1,0:T(8,128)(2,1)S(1)} %get-tuple-element.106), channel_id=1, source_target_pairs={{0,16},{4,20},{8,24},{12,28},{16,0},{20,4},{24,8},{28,12},{1,17},{... | collective-permute-start | bytes 221192 | tf_op jit(solution)/shard_map/ppermute | solution.py:111
  162.0 7.0 %collective-permute-start.34 = (bf16[144,256]{1,0:T(8,128)(2,1)S(1)}, bf16[144,256]{1,0:T(8,128)(2,1)S(1)}, u32[]{:S(2)}, u32[]{:S(2)}) collective-permute-start(bf16[144,256]{1,0:T(8,128)(2,1)S(1)} %get-tuple-element.107), channel_id=1, source_target_pairs={{0,20},{4,16},{8,28},{12,24},{16,4},{20,0},{24,12},{28,8},{1,21},{... | collective-permute-start | bytes 221192 | tf_op jit(solution)/shard_map/ppermute | solution.py:111
  164.4 7.1 %collective-permute-start.36 = (bf16[144,256]{1,0:T(8,128)(2,1)S(1)}, bf16[144,256]{1,0:T(8,128)(2,1)S(1)}, u32[]{:S(2)}, u32[]{:S(2)}) collective-permute-start(bf16[144,256]{1,0:T(8,128)(2,1)S(1)} %get-tuple-element.109), channel_id=1, source_target_pairs={{0,28},{4,24},{8,20},{12,16},{16,12},{20,8},{24,4},{28,0},{1,29},{... | collective-permute-start | bytes 221192 | tf_op jit(solution)/shard_map/ppermute | solution.py:111
  172.6 8.1 %collective-permute-start.38 = (bf16[384,256]{1,0:T(8,128)(2,1)S(1)}, bf16[384,256]{1,0:T(8,128)(2,1)S(1)}, u32[]{:S(2)}, u32[]{:S(2)}) collective-permute-start(bf16[384,256]{1,0:T(8,128)(2,1)S(1)} %shard_map.201.refs_0_.p0), channel_id=1, source_target_pairs={{0,2},{1,3},{2,0},{3,1},{4,6},{5,7},{6,4},{7,5},{8,10},{9,11},{10,... | collective-permute-start | bytes 589832 | tf_op jit(solution)/shard_map/ppermute | solution.py:36
  173.2 7.9 %collective-permute-start.51 = (bf16[384,256]{1,0:T(8,128)(2,1)S(1)}, bf16[384,256]{1,0:T(8,128)(2,1)S(1)}, u32[]{:S(2)}, u32[]{:S(2)}) collective-permute-start(bf16[384,256]{1,0:T(8,128)(2,1)S(1)} %shard_map.203.refs_4_.p0), channel_id=1, source_target_pairs={{0,1},{1,0},{2,3},{3,2},{4,5},{5,4},{6,7},{7,6},{8,9},{9,8},{10,11... | collective-permute-start | bytes 589832 | tf_op jit(solution)/shard_map/ppermute | solution.py:36
  173.2 7.9 %collective-permute-start.53 = (bf16[384,256]{1,0:T(8,128)(2,1)S(1)}, bf16[384,256]{1,0:T(8,128)(2,1)S(1)}, u32[]{:S(2)}, u32[]{:S(2)}) collective-permute-start(bf16[384,256]{1,0:T(8,128)(2,1)S(1)} %collective-permute-done.52.refs_6_.p2), channel_id=1, source_target_pairs={{0,1},{1,0},{2,3},{3,2},{4,5},{5,4},{6,7},{7,6},{8,9},{9,8},{10,11... | collective-permute-start | bytes 589832 | tf_op jit(solution)/shard_map/ppermute | solution.py:36
  180.4 7.6 %collective-permute-start.37 = (bf16[384,256]{1,0:T(8,128)(2,1)S(1)}, bf16[384,256]{1,0:T(8,128)(2,1)S(1)}, u32[]{:S(2)}, u32[]{:S(2)}) collective-permute-start(bf16[384,256]{1,0:T(8,128)(2,1)S(1)} %shard_map.201.refs_0_.p0), channel_id=1, source_target_pairs={{0,1},{1,0},{2,3},{3,2},{4,5},{5,4},{6,7},{7,6},{8,9},{9,8},{10,11... | collective-permute-start | bytes 589832 | tf_op jit(solution)/shard_map/ppermute | solution.py:36
  180.7 7.4 %collective-permute-start.39 = (bf16[384,256]{1,0:T(8,128)(2,1)S(1)}, bf16[384,256]{1,0:T(8,128)(2,1)}, u32[]{:S(2)}, u32[]{:S(2)}) collective-permute-start(bf16[384,256]{1,0:T(8,128)(2,1)S(1)} %collective-permute-done.38.refs_2_.p2), channel_id=1, source_target_pairs={{0,1},{1,0},{2,3},{3,2},{4,5},{5,4},{6,7},{7,6},{8,9},{9,8},{10,11... | collective-permute-start | bytes 589832 | tf_op jit(solution)/shard_map/ppermute | solution.py:36
  183.1 19.9 %all-to-all-start.1 = ((bf16[8,256,128]{2,1,0:T(8,128)(2,1)}), bf16[8,256,128]{2,1,0:T(8,128)(2,1)}, u32[]{:S(2)}, u32[]{:S(2)}) async-start(bf16[8,256,128]{2,1,0:T(8,128)(2,1)} %shard_map.208), calls=%async_computation.1 | async-start | bytes 1048576 | tf_op jit(solution)/shard_map/all_to_all | solution.py:122
  197.8 22.0 %collective-permute-start.60 = (f32[30,256]{1,0:T(8,128)S(1)}, f32[30,256]{1,0:T(8,128)S(1)}, u32[]{:S(2)}, u32[]{:S(2)}) collective-permute-start(f32[30,256]{1,0:T(8,128)S(1)} %slice.288), channel_id=1, source_target_pairs={{4,0},{8,4},{12,8},{16,12},{20,16},{24,20},{28,24},{5,1},{9,5},{13... | collective-permute-start | bytes 92168 | tf_op jit(solution)/shard_map/ppermute | solution.py:47
  203.0 21.1 %all-to-all-start = ((bf16[8,256,128]{2,1,0:T(8,128)(2,1)}), bf16[8,256,128]{2,1,0:T(8,128)(2,1)S(1)}, u32[]{:S(2)}, u32[]{:S(2)}) async-start(bf16[8,256,128]{2,1,0:T(8,128)(2,1)} %shard_map.207), calls=%async_computation | async-start | bytes 1048576 | tf_op jit(solution)/shard_map/all_to_all | solution.py:122
  (77 other events, 732.9 us)
